TPU v7x, 32 devices: a whole 2x2x4 slice. The times are simulated.
32 devices in a mesh: grp: 2 (over y), ep: 8 (over z, x), tp: 2 (over core).
Axes of the slice: x: 2, y: 2, z: 4, core: 2. Of those that a mesh axis runs over, the one named last changes fastest.
Arguments:
- tokens: bfloat16 [512, 2048], P(('grp', 'ep'), 'tp'), parts along dimension 0, may hold values from -6 to 6
- gain: float32 [2048], replicated, may hold values from 0.1 to 1.9
- routes: int32 [512, 4], P(('grp', 'ep')), parts along dimension 0, may hold values from 0 to 7, all different within a row; in each aligned block of 32 rows (0 to 31, 32 to 63, ...) at most 32 rows name the same one
- weights: float32 [512, 4], P(('grp', 'ep')), parts along dimension 0, may hold values from 0.05 to 1
- w_gate: bfloat16 [8, 2048, 6144], P('ep', None, 'tp'), may hold values from -0.125 to 0.125
- w_up: bfloat16 [8, 2048, 6144], P('ep', None, 'tp'), may hold values from -0.125 to 0.125
- w_down: bfloat16 [8, 6144, 2048], P('ep', 'tp'), may hold values from -0.078125 to 0.078125
Outputs:
- mixed: bfloat16 [512, 2048], P(('grp', 'ep'), 'tp'), parts along dimension 0
There are 2 independent parts, one for each index of `grp`. A program takes and returns all parts, laid end to end along the dimension named above; an argument that names none is the same for every part. Nothing has to cross between parts.
Inputs may be any that keep to these rules, and one draw needn't show every extreme that they name: `routes`: each row names 4 different experts. Among the rows of one device no expert is named by more than 32 rows, a bound that some block reaches.
All inputs are finite; a program needn't handle non-finite values.
Results may differ from a plain program's by a relative error of at most 0.019.
Values may be sent and summed in bfloat16 or wider, within the bound.
No kernel may reach another device: no remote copies, remote signals or barrier semaphores. Data moves between devices by JAX's collectives and lax.ppermute only.
A program may use at most 128 MiB of HBM per device.

v0:
```python
import jax
import jax.numpy as jnp
from jax import lax
from jax.sharding import PartitionSpec as P

epsilon = 1e-05


def expert_rows(chosen, gate_w, up_w, down_w):
    gate_val = jnp.dot(chosen, gate_w, preferred_element_type=jnp.float32)
    up_val = jnp.dot(chosen, up_w, preferred_element_type=jnp.float32)
    hidden = (jax.nn.silu(gate_val) * up_val).astype(jnp.bfloat16)
    partial_value = jnp.dot(hidden, down_w, preferred_element_type=jnp.float32).astype(jnp.bfloat16)
    return (
        lax.psum_scatter(partial_value, "tp", scatter_dimension=1, tiled=True)
        .astype(jnp.float32)
        .astype(jnp.bfloat16)
    )


def on_device(tokens, gain, routes, weights, w_gate, w_up, w_down):
    groups = lax.axis_size("ep")
    shards = lax.axis_size("tp")
    tok_rows, top_count = routes.shape
    capacity = min(tok_rows, 2 * tok_rows * top_count // groups)
    gate_w, up_w, down_w = (w_gate[0], w_up[0], w_down[0])
    values = tokens.astype(jnp.float32)
    own_width = values.shape[1]
    width = own_width * shards
    totals = lax.psum((jnp.sum(values, axis=1), jnp.sum(values * values, axis=1)), "tp")
    average = totals[0] / width
    spread = totals[1] / width - average * average
    local_gain = lax.dynamic_slice_in_dim(gain, lax.axis_index("tp") * own_width, own_width)
    normed = (
        (values - average[:, None]) * lax.rsqrt(spread[:, None] + epsilon) * local_gain
    ).astype(jnp.bfloat16)
    pair_expert = routes.reshape(-1)
    pair_token = jnp.arange(tok_rows * top_count, dtype=jnp.int32) // top_count
    member = (pair_expert[:, None] == jnp.arange(groups, dtype=jnp.int32)[None, :]).astype(
        jnp.int32
    )
    earlier = jnp.cumsum(member, axis=0) - member
    position = pair_expert * capacity + jnp.sum(earlier * member, axis=1)
    row_width = normed.shape[1]
    outbox = (
        jnp.zeros((groups * capacity, row_width), jnp.bfloat16).at[position].set(normed[pair_token])
    )
    outbox = outbox.reshape(groups, capacity, row_width)
    arrived = lax.all_gather(
        lax.all_to_all(outbox, "ep", split_axis=0, concat_axis=0, tiled=True),
        "tp",
        axis=2,
        tiled=True,
    )
    count = arrived.shape[1]
    flat_rows = arrived.reshape(groups * count, arrived.shape[2])
    served = expert_rows(flat_rows, gate_w, up_w, down_w).reshape(groups, count, -1)
    returned = lax.all_to_all(served, "ep", split_axis=0, concat_axis=0, tiled=True)
    picked = (
        returned.reshape(groups * capacity, -1)[position]
        .reshape(tok_rows, top_count, -1)
        .astype(jnp.float32)
    )
    return jnp.sum(picked * weights[:, :, None], axis=1).astype(jnp.bfloat16)


def solution(mesh):
    in_specs = (
        P(("grp", "ep"), "tp"),
        P(),
        P(("grp", "ep"), None),
        P(("grp", "ep"), None),
        P("ep", None, "tp"),
        P("ep", None, "tp"),
        P("ep", "tp", None),
    )
    out_specs = P(("grp", "ep"), "tp")
    return jax.shard_map(
        on_device, mesh=mesh, in_specs=in_specs, out_specs=out_specs, check_vma=False
    )
```

profile of v0, /device:TPU:0, one launch (start us, length us, event | category | flops | bytes accessed | tf_op | source)
XLA Modules:
  0.0 112.8 jit_solution(12843658255355050022)
XLA Ops:
  6.5 0.8 copy.12
  7.3 0.7 broadcast_multiply_fusion
  8.0 1.0 convert_reduce_fusion
  9.0 0.1 eq.15
  9.1 0.1 fusion.24
  9.2 0.2 reduce_window_sum.11
  9.3 0.2 select_reduce_fusion
  9.5 0.1 copy.11
  9.6 0.1 mul.57
  9.7 2.6 %all-reduce = (f32[32]{0:T(128)S(1)}, f32[32]{0:T(128)S(1)}) all-reduce(f32[32]{0:T(128)S(1)} %get-tuple-element.6, f32[32]{0:T(128)S(1)} %get-tuple-element.5), channel_id=1, replica_groups=mesh['grp'=2,'ep'=8,'tp'=2] {'tp'}, use_global_device_ids=true, to_apply=%region_5.6 | all-reduce | flops 64 | bytes 512 | tf_op jit(solution)/shard_map/psum | solution.py:30
  12.4 0.7 dynamic_slice.3
  13.1 0.9 fusion.22
  14.0 2.2 %scatter_custom_fusion = bf16[256,1024]{1,0:T(8,128)(2,1)S(1)} fusion(s32[128]{0:T(128)S(1)} %fusion.26, bf16[32,1024]{1,0:T(8,128)(2,1)S(1)} %fusion.22, s32[1024]{0:T(1024)S(1)} %pad_clamp_fusion.1, bf16[]{:T(256)} %constant.34.clone.1), kind=kCustom, calls=%fused_computation.13 | custom fusion | bytes 524290 | tf_op jit(solution)/shard_map/scatter | solution.py:46
  16.2 21.8 %all_to_all.10 = bf16[8,32,1024]{2,1,0:T(8,128)(2,1)} all-to-all(bf16[8,32,1024]{2,1,0:T(8,128)(2,1)S(1)} %bitcast.32), channel_id=1, replica_groups=mesh['grp'=2,'ep'=8,'tp'=2] {'ep'}, dimensions={0} | all-to-all | bytes 1048576 | tf_op jit(solution)/shard_map/all_to_all | solution.py:50
  38.1 8.2 %all-gather.2.cloned.1.call-done = bf16[8,32,2048]{2,1,0:T(8,128)(2,1)} async-done(((bf16[8,32,1024]{2,1,0:T(8,128)(2,1)}), bf16[8,32,2048]{2,1,0:T(8,128)(2,1)}) %all-gather.2.cloned.1.call-update) | async-done | bytes 1048592 | tf_op jit(solution)/shard_map/all_gather | solution.py:49
  46.3 10.1 %fusion.4 = f32[256,3072]{1,0:T(8,128)} fusion(bf16[256,2048]{1,0:T(8,128)(2,1)} %bitcast.34, bf16[1,2048,3072]{2,1,0:T(8,128)(2,1)} %param.11), kind=kOutput, calls=%fused_computation.7 | convolution fusion | flops 3221225472 | bytes 16777216 | tf_op jit(solution)/shard_map/dot_general | solution.py:10
  56.4 17.0 %fusion.12 = bf16[256,2048]{1,0:T(8,128)(2,1)} fusion(bf16[1,3072,2048]{2,1,0:T(8,128)(2,1)} %param.13, bf16[256,2048]{1,0:T(8,128)(2,1)S(1)} %bitcast.35, bf16[1,2048,3072]{2,1,0:T(8,128)(2,1)} %param.12, f32[256,3072]{1,0:T(8,128)} %fusion.4), kind=kOutput, calls=%fused_computation.11 | convolution fusion | flops 6447693824 | bytes 30408704 | tf_op jit(solution)/shard_map/dot_general | solution.py:13
  73.5 9.7 %reduce-scatter.2.cloned.1.call-done = bf16[256,1024]{1,0:T(8,128)(2,1)} async-done(((bf16[256,2048]{1,0:T(8,128)(2,1)}), bf16[256,1024]{1,0:T(8,128)(2,1)}) %reduce-scatter.2.cloned.1.call-update) | async-done | bytes 524304 | tf_op jit(solution)/shard_map/reduce_scatter | solution.py:15
  83.2 5.8 %all-to-all-start.1 = ((bf16[8,32,1024]{2,1,0:T(8,128)(2,1)}), bf16[8,32,1024]{2,1,0:T(8,128)(2,1)S(1)}, u32[]{:S(2)}, u32[]{:S(2)}) async-start(bf16[8,32,1024]{2,1,0:T(8,128)(2,1)} %bitcast.33), calls=%async_computation.2 | async-start | bytes 1048576 | tf_op jit(solution)/shard_map/all_to_all | solution.py:58
  88.9 0.1 copy.13
  89.0 14.8 %all-to-all-done.1 = bf16[8,32,1024]{2,1,0:T(8,128)(2,1)S(1)} async-done(((bf16[8,32,1024]{2,1,0:T(8,128)(2,1)}), bf16[8,32,1024]{2,1,0:T(8,128)(2,1)S(1)}, u32[]{:S(2)}, u32[]{:S(2)}) %all-to-all-start.1) | async-done | bytes 524320 | tf_op jit(solution)/shard_map/all_to_all | solution.py:58
  103.9 0.9 gather_fusion
  104.7 0.2 reshape.98
  104.9 1.0 multiply_reduce_fusion
  (13 shorter events, 0.1 us)
Async XLA Ops:
  6.5 39.8 %all-gather.2.cloned.1.call-start = ((), (), s32[]{:S(2)}) async-start(), calls=%async_computation.3 | async-start | bytes 1572864 | tf_op jit(solution)/shard_map/all_gather | solution.py:49
  38.1 45.1 %reduce-scatter.2.cloned.1.call-start = ((), (), s32[]{:S(2)}) async-start(), calls=%async_computation.4 | async-start | bytes 1572864 | tf_op jit(solution)/shard_map/reduce_scatter | solution.py:15
  46.3 10.1 %copy-start.1 = (bf16[8,32,2048]{2,1,0:T(8,128)(2,1)S(1)}, bf16[8,32,2048]{2,1,0:T(8,128)(2,1)}, u32[]{:S(2)}) copy-start(bf16[8,32,2048]{2,1,0:T(8,128)(2,1)} %all-gather.2.cloned.1.call-done) | copy-start | bytes 3145732
  56.4 32.5 %copy-start = (f32[32,4]{0,1:T(4,128)S(1)}, f32[32,4]{0,1:T(4,128)}, u32[]{:S(2)}) copy-start(f32[32,4]{0,1:T(4,128)} %param.10) | copy-start | bytes 1540
  83.2 20.7 %all-to-all-start.1 = ((bf16[8,32,1024]{2,1,0:T(8,128)(2,1)}), bf16[8,32,1024]{2,1,0:T(8,128)(2,1)S(1)}, u32[]{:S(2)}, u32[]{:S(2)}) async-start(bf16[8,32,1024]{2,1,0:T(8,128)(2,1)} %bitcast.33), calls=%async_computation.2 | async-start | bytes 1048576 | tf_op jit(solution)/shard_map/all_to_all | solution.py:58
Sparse Core Ops, SparseCore 0:
  38.2 8.0 all-gather.1
  73.6 9.5 reduce-scatter.1
where the time goes:
time: 113 us
  waiting for transfers between devices  32.8 us (29%)
  matrix products  27.1 us (24%)
  blocking collectives  24.5 us (22%)
  between operations  13.5 us (12%)
  starting transfers between devices  5.82 us (5%)
  local copies, waits for them, and re-layouts  5.08 us (4%)
  other arithmetic  4.06 us (4%)
    all_to_all x1, blocking collectives, on_device(): lax.all_to_all(outbox, 'ep', split_axis=0, concat_axis=0, tiled=True)  21.8 us
    dot_general x1, matrix products, expert_rows(): jnp.dot(hidden, down_w, preferred_element_type=jnp.float32)  17 us
    all_to_all x1, waiting for transfers between devices, on_device(): lax.all_to_all(served, 'ep', split_axis=0, concat_axis=0, tiled=True)  14.8 us
    dot_general x1, matrix products, expert_rows(): gate_val = jnp.dot(chosen, gate_w, preferred_element_type=jnp.float32)  10.1 us
    reduce_scatter x1, waiting for transfers between devices, expert_rows(): lax.psum_scatter(partial_value, 'tp', scatter_dimension=1, tiled=True)  9.7 us
    all_gather x1, waiting for transfers between devices, on_device(): lax.all_gather(lax.all_to_all(outbox, 'ep', split_axis=0, concat_axis=0,...  8.21 us
    all_to_all x1, starting transfers between devices, on_device(): lax.all_to_all(served, 'ep', split_axis=0, concat_axis=0, tiled=True)  5.78 us
    psum x1, blocking collectives, on_device(): lax.psum((jnp.sum(values, axis=1), jnp.sum(values * values, axis=1)), 'tp')  2.63 us
  transfers between devices with their start and end apart: 3, of which 3 were waited for; matrix products, arithmetic and copies ran while one was open for 0% of the time, Pallas kernels for 0%

commit v1 on v0

v1 whole, which is shorter than its diff:
```python
import jax
import jax.numpy as jnp
from jax import lax
from jax.experimental import pallas as pl
from jax.experimental.pallas import tpu as pltpu
from jax.sharding import PartitionSpec as P

EPS = 1e-05
LANES = 128
MIB = 1 << 20


def vmem():
    return pl.BlockSpec(memory_space=pltpu.VMEM)


def hbm():
    return pl.BlockSpec(memory_space=pltpu.HBM)


def in_hbm(value):
    return pltpu.with_memory_space_constraint(value, pltpu.HBM)


def in_vmem(value):
    return pltpu.with_memory_space_constraint(value, pltpu.VMEM)


def block_of(size, most):
    return max(b for b in range(LANES, most + 1, LANES) if size % b == 0)


def swap(value, axis, bit):
    return lax.ppermute(value, axis, [(i, i ^ bit) for i in range(lax.axis_size(axis))])


def prepare_body(tokens_hbm, routes_hbm, weights_hbm, out, tokens, routes, weights, sem):
    copies = [
        pltpu.make_async_copy(a, b, sem.at[i])
        for i, (a, b) in enumerate(
            ((routes_hbm, routes), (weights_hbm, weights), (tokens_hbm, tokens))
        )
    ]
    for copy in copies:
        copy.start()
    copies[0].wait()
    copies[1].wait()
    rows, width = tokens.shape
    lane = lax.broadcasted_iota(jnp.int32, (LANES, rows), 0)
    share = jnp.zeros((LANES, rows), jnp.float32)
    for k in range(routes.shape[0]):
        share = share + jnp.where(routes[k : k + 1, :] == lane, weights[k : k + 1, :], 0.0)
    out[:, width:] = share.T.astype(jnp.bfloat16)
    copies[2].wait()
    out[:, :width] = tokens[...]


def prepare(tokens, routes, weights):
    rows, width = tokens.shape
    arrays = (tokens, routes.T, weights.T)
    return pl.pallas_call(
        prepare_body,
        out_shape=jax.ShapeDtypeStruct((rows, width + LANES), jnp.bfloat16),
        in_specs=[hbm()] * 3,
        out_specs=vmem(),
        scratch_shapes=[pltpu.VMEM(a.shape, a.dtype) for a in arrays]
        + [pltpu.SemaphoreType.DMA((3,))],
        compiler_params=pltpu.CompilerParams(vmem_limit_bytes=2 * MIB),
        name="prepare",
    )(*(in_hbm(a) for a in arrays))


def fetch_body(source, target, sem):
    copy = pltpu.make_async_copy(source, target, sem)
    copy.start()
    copy.wait()


def fetch(weight, after):
    del after
    return pl.pallas_call(
        fetch_body,
        out_shape=pltpu.VMEM(weight.shape, weight.dtype),
        in_specs=[hbm()],
        out_specs=vmem(),
        scratch_shapes=[pltpu.SemaphoreType.DMA],
        cost_estimate=pl.CostEstimate(
            flops=4 * 10**9, transcendentals=0, bytes_accessed=2 * weight.size
        ),
        compiler_params=pltpu.CompilerParams(vmem_limit_bytes=MIB),
        name="fetch",
    )(in_hbm(weight))


def expert_body(own, other, gain_hbm, w_gate, w_up, down, *rest, pieces, width, fetches):
    if fetches:
        keep, send, w_down, normed, hidden, gain, sem = rest
        copy = pltpu.make_async_copy(down, w_down, sem.at[1])
        copy.start()
    else:
        keep, send, normed, hidden, gain, sem = rest
        w_down = down
    gain_copy = pltpu.make_async_copy(gain_hbm, gain, sem.at[0])
    gain_copy.start()
    core, index = lax.axis_index("tp"), lax.axis_index("ep")
    at = pl.multiple_of(core * width, LANES)
    far = pl.multiple_of((pieces - 1 - core) * width, LANES)
    features = pieces * width
    mine = own[:, :width].astype(jnp.float32)
    theirs = other[:, :width].astype(jnp.float32)
    average = (
        jnp.sum(mine, axis=1, keepdims=True) + jnp.sum(theirs, axis=1, keepdims=True)
    ) / features
    mine = mine - average
    theirs = theirs - average
    spread = (
        jnp.sum(mine * mine, axis=1, keepdims=True)
        + jnp.sum(theirs * theirs, axis=1, keepdims=True)
    ) / features
    scale = lax.rsqrt(spread + EPS)
    gain_copy.wait()
    normed[:, pl.ds(at, width)] = (mine * scale * gain[:, pl.ds(at, width)]).astype(jnp.bfloat16)
    normed[:, pl.ds(far, width)] = (theirs * scale * gain[:, pl.ds(far, width)]).astype(
        jnp.bfloat16
    )
    share = own[:, width:].astype(jnp.float32)
    lane = lax.broadcasted_iota(jnp.int32, share.shape, 1)
    share = jnp.sum(jnp.where(lane == index, share, 0.0), axis=1, keepdims=True)
    chosen = normed[...]
    units = w_gate.shape[1]
    step = block_of(units, 256)
    for n in range(0, units, step):
        gate_val = jnp.dot(chosen, w_gate[:, n : n + step], preferred_element_type=jnp.float32)
        up_val = jnp.dot(chosen, w_up[:, n : n + step], preferred_element_type=jnp.float32)
        hidden[:, n : n + step] = (gate_val / (1.0 + jnp.exp(-gate_val)) * up_val).astype(
            jnp.bfloat16
        )
    if fetches:
        copy.wait()
    middle = hidden[...]
    step = block_of(width, 256)
    for target, base in ((send, far), (keep, at)):
        for n in range(0, width, step):
            part = jnp.dot(
                middle,
                w_down[:, pl.ds(pl.multiple_of(base + n, LANES), step)],
                preferred_element_type=jnp.float32,
            )
            target[:, n : n + step] = (part * share).astype(target.dtype)


def expert(own, other, gain, w_gate, w_up, w_down, fetches):
    width = own.shape[1] - LANES
    rows = own.shape[0]
    features, units = w_gate.shape
    body = lambda *refs: expert_body(
        *refs, pieces=features // width, width=width, fetches=fetches
    )
    rows_out = jax.ShapeDtypeStruct((rows, width), jnp.bfloat16)
    out_shape = [rows_out, rows_out]
    if fetches:
        out_shape.append(pltpu.VMEM(w_down.shape, w_down.dtype))
    return pl.pallas_call(
        body,
        out_shape=out_shape,
        in_specs=[vmem()] * 2 + [hbm()] + [vmem()] * 2 + [hbm() if fetches else vmem()],
        out_specs=[vmem()] * len(out_shape),
        scratch_shapes=[
            pltpu.VMEM((rows, features), jnp.bfloat16),
            pltpu.VMEM((rows, units), jnp.bfloat16),
            pltpu.VMEM((1, features), jnp.float32),
            pltpu.SemaphoreType.DMA((2,)),
        ],
        cost_estimate=pl.CostEstimate(
            flops=6 * rows * features * units,
            transcendentals=rows * units,
            bytes_accessed=6 * features * units,
        ),
        compiler_params=pltpu.CompilerParams(vmem_limit_bytes=12 * MIB),
        name="expert",
    )(
        own,
        other,
        in_hbm(gain[None, :]),
        in_vmem(w_gate),
        in_vmem(w_up),
        in_hbm(w_down) if fetches else in_vmem(w_down),
    )


def add(a, b):
    return (a.astype(jnp.float32) + b.astype(jnp.float32)).astype(jnp.bfloat16)


def on_device_pair(tokens, gain, routes, weights, w_gate, w_up, w_down):
    groups = lax.axis_size("ep")
    gathered = prepare(tokens, routes, weights)
    bits = []
    bit = groups // 2
    while bit > 1:
        gathered = jnp.concatenate([gathered, swap(gathered, "ep", bit)], axis=0)
        bits.append(bit)
        bit //= 2
    gate_w = fetch(w_gate[0], None)
    up_w = fetch(w_up[0], None)
    near = gathered
    near_other = swap(near, "tp", 1)
    beside = swap(near, "ep", 1)
    near_keep, near_send, down_w = expert(near, near_other, gain, gate_w, up_w, w_down[0], True)
    beside_other = swap(beside, "tp", 1)
    beside_keep, beside_send = expert(beside, beside_other, gain, gate_w, up_w, down_w, False)
    beside_sum = add(beside_keep, swap(beside_send, "tp", 1))
    near_sum = add(near_keep, swap(near_send, "tp", 1))
    total = add(near_sum, swap(beside_sum, "ep", 1))
    for bit in reversed(bits):
        half = total.shape[0] // 2
        total = add(total[:half], swap(total[half:], "ep", bit))
    return total


def on_device_any(tokens, gain, routes, weights, w_gate, w_up, w_down):
    groups = lax.axis_size("ep")
    width = tokens.shape[1]
    rows = prepare(tokens, routes, weights)
    bits = [1 << i for i in reversed(range(groups.bit_length() - 1))]
    for bit in bits:
        rows = jnp.concatenate([rows, swap(rows, "ep", bit)], axis=0)
    lane = jnp.arange(LANES, dtype=jnp.int32)[None, :]
    share = jnp.where(lane == lax.axis_index("ep"), rows[:, width:].astype(jnp.float32), 0.0)
    share = jnp.sum(share, axis=1, keepdims=True)
    values = lax.all_gather(rows[:, :width], "tp", axis=1, tiled=True).astype(jnp.float32)
    values = values - jnp.mean(values, axis=1, keepdims=True)
    spread = jnp.mean(values * values, axis=1, keepdims=True)
    chosen = (values * lax.rsqrt(spread + EPS) * gain).astype(jnp.bfloat16)
    gate_val = jnp.dot(chosen, w_gate[0], preferred_element_type=jnp.float32)
    up_val = jnp.dot(chosen, w_up[0], preferred_element_type=jnp.float32)
    hidden = (jax.nn.silu(gate_val) * up_val).astype(jnp.bfloat16)
    part = jnp.dot(hidden, w_down[0], preferred_element_type=jnp.float32)
    total = lax.psum_scatter(
        (part * share).astype(jnp.bfloat16), "tp", scatter_dimension=1, tiled=True
    )
    for bit in reversed(bits):
        half = total.shape[0] // 2
        total = add(total[:half], swap(total[half:], "ep", bit))
    return total


def solution(mesh):
    in_specs = (
        P(("grp", "ep"), "tp"),
        P(),
        P(("grp", "ep"), None),
        P(("grp", "ep"), None),
        P("ep", None, "tp"),
        P("ep", None, "tp"),
        P("ep", "tp", None),
    )
    on_device = on_device_pair if mesh.shape["tp"] == 2 else on_device_any
    return jax.shard_map(
        on_device,
        mesh=mesh,
        in_specs=in_specs,
        out_specs=P(("grp", "ep"), "tp"),
        check_vma=False,
    )
```

time: 113 us -> 62.9 us (0.56)
  matrix products: 27.1 us -> 0 us
  Pallas kernels: 0 us -> 26.1 us
  blocking collectives: 24.5 us -> 0 us
  between operations: 13.5 us -> 0.12 us
  waiting for transfers between devices: 32.8 us -> 21.7 us
  starting transfers between devices: 5.82 us -> 13.7 us
  local copies, waits for them, and re-layouts: 5.08 us -> 0.02 us
  other arithmetic: 4.06 us -> 0.91 us
    dot_general x2 -> x0, matrix products: 27.1 us -> none  [the longest x1 17 us: expert_rows(): jnp.dot(hidden, down_w, preferred_element_type=jnp.float32)]
    pallas_call x0 -> x5, Pallas kernels: none -> 26.1 us  [the longest x2 16 us: expert(): pl.pallas_call(body, out_shape=out_shape, in_specs=[vmem()] * 2 + [hbm()]...]
    all_to_all x1 -> x0, blocking collectives: 21.8 us -> none  [on_device(): lax.all_to_all(outbox, 'ep', split_axis=0, concat_axis=0, tiled=True)]
    ppermute x0 -> x10, waiting for transfers between devices: none -> 21.7 us  [swap(): lax.ppermute(value, axis, [(i, i ^ bit) for i in range(lax.axis_size(axis...]
    all_to_all x1 -> x0, waiting for transfers between devices: 14.8 us -> none  [on_device(): lax.all_to_all(served, 'ep', split_axis=0, concat_axis=0, tiled=True)]
    ppermute x0 -> x10, starting transfers between devices: none -> 13.7 us  [swap(): lax.ppermute(value, axis, [(i, i ^ bit) for i in range(lax.axis_size(axis...]
    reduce_scatter x1 -> x0, waiting for transfers between devices: 9.7 us -> none  [expert_rows(): lax.psum_scatter(partial_value, 'tp', scatter_dimension=1, tiled=True)]
    all_gather x1 -> x0, waiting for transfers between devices: 8.21 us -> none  [on_device(): lax.all_gather(lax.all_to_all(outbox, 'ep', split_axis=0, concat_axis=0,...]
  transfers between devices with their start and end apart: 3 -> 10, of which waited for: 3 -> 6; matrix products, arithmetic and copies ran while one was open for 0% -> 0% of each run, Pallas kernels for 0% -> 30%
where the time goes in v1:
time: 62.9 us; the launch traced here: 62.6 us
  Pallas kernels  26.1 us (41%)
  waiting for transfers between devices  21.7 us (34%)
  starting transfers between devices  13.7 us (22%)
  other arithmetic  0.91 us (1%)
    ppermute x10, waiting for transfers between devices, swap(): lax.ppermute(value, axis, [(i, i ^ bit) for i in range(lax.axis_size(axis...  21.7 us
    pallas_call x2, Pallas kernels, expert(): pl.pallas_call(body, out_shape=out_shape, in_specs=[vmem()] * 2 + [hbm()]...  16 us
    ppermute x10, starting transfers between devices, swap(): lax.ppermute(value, axis, [(i, i ^ bit) for i in range(lax.axis_size(axis...  13.7 us
    pallas_call x2, Pallas kernels, fetch(): pl.pallas_call(fetch_body, out_shape=pltpu.VMEM(weight.shape, weight.dtyp...  9.17 us
  transfers between devices with their start and end apart: 10, of which 6 were waited for; matrix products, arithmetic and copies ran while one was open for 0% of the time, Pallas kernels for 30%

profile of v1, /device:TPU:0, one launch (start us, length us, event | category | flops | bytes accessed | tf_op | source)
XLA Modules:
  0.0 62.6 jit_solution(14952777267214245349)
XLA Ops:
  0.0 0.9 %prepare.1 = bf16[32,1152]{1,0:T(8,128)(2,1)S(1)} custom-call(bf16[32,1024]{1,0:T(8,128)(2,1)} %tokens_hbm.1, s32[4,32]{1,0:T(4,128)} %bitcast.11, f32[4,32]{1,0:T(4,128)} %bitcast.12), custom_call_target="tpu_custom_call" | custom-call | tf_op jit(solution)/shard_map/prepare/pallas_call | solution.py:61
  0.9 4.1 %collective-permute-start = (bf16[32,1152]{1,0:T(8,128)(2,1)S(1)}, bf16[32,1152]{1,0:T(8,128)(2,1)S(1)}, u32[]{:S(2)}, u32[]{:S(2)}) collective-permute-start(bf16[32,1152]{1,0:T(8,128)(2,1)S(1)} %prepare.1), channel_id=1, source_target_pairs={{0,8},{2,10},{4,12},{6,14},{8,0},{10,2},{12,4},{14,6},{1,9},{3,11}... | collective-permute-start | bytes 221192 | tf_op jit(solution)/shard_map/ppermute | solution.py:34
  5.0 3.9 %collective-permute-done = bf16[32,1152]{1,0:T(8,128)(2,1)S(1)} collective-permute-done((bf16[32,1152]{1,0:T(8,128)(2,1)S(1)}, bf16[32,1152]{1,0:T(8,128)(2,1)S(1)}, u32[]{:S(2)}, u32[]{:S(2)}) %collective-permute-start) | collective-permute-done | bytes 73760 | tf_op jit(solution)/shard_map/ppermute | solution.py:34
  9.0 0.7 %collective-permute-start.1 = (bf16[64,1152]{1,0:T(8,128)(2,1)S(1)}, bf16[64,1152]{1,0:T(8,128)(2,1)S(1)}, u32[]{:S(2)}, u32[]{:S(2)}) collective-permute-start(bf16[64,1152]{1,0:T(8,128)(2,1)S(1)} %pad_maximum_fusion.1), channel_id=1, source_target_pairs={{0,4},{2,6},{4,0},{6,2},{8,12},{10,14},{12,8},{14,10},{1,5},{3,7},... | collective-permute-start | bytes 442376 | tf_op jit(solution)/shard_map/ppermute | solution.py:34
  9.7 4.6 %fetch.2.refs_3_ = bf16[2048,3072]{1,0:T(8,128)(2,1)S(1)} custom-call(bf16[2048,3072]{1,0:T(8,128)(2,1)} %bitcast.6), custom_call_target="tpu_custom_call" | custom-call | flops 4000000000 | bytes 12582912 | tf_op jit(solution)/shard_map/fetch/pallas_call | solution.py:81
  14.3 0.1 collective-permute-start.2
  14.4 1.6 %collective-permute-start.4 = (bf16[128,1152]{1,0:T(8,128)(2,1)S(1)}, bf16[128,1152]{1,0:T(8,128)(2,1)S(1)}, u32[]{:S(2)}, u32[]{:S(2)}) collective-permute-start(bf16[128,1152]{1,0:T(8,128)(2,1)S(1)} %pad_maximum_fusion.refs_0_), channel_id=1, source_target_pairs={{0,2},{2,0},{4,6},{6,4},{8,10},{10,8},{12,14},{14,12},{1,3},{3,1},... | collective-permute-start | bytes 884744 | tf_op jit(solution)/shard_map/ppermute | solution.py:34
  16.0 4.6 %fetch.3.refs_4_ = bf16[2048,3072]{1,0:T(8,128)(2,1)S(1)} custom-call(bf16[2048,3072]{1,0:T(8,128)(2,1)} %bitcast.7), custom_call_target="tpu_custom_call" | custom-call | flops 4000000000 | bytes 12582912 | tf_op jit(solution)/shard_map/fetch/pallas_call | solution.py:81
  20.6 3.2 %collective-permute-done.4.refs_0_ = bf16[128,1152]{1,0:T(8,128)(2,1)S(1)} collective-permute-done((bf16[128,1152]{1,0:T(8,128)(2,1)S(1)}, bf16[128,1152]{1,0:T(8,128)(2,1)S(1)}, u32[]{:S(2)}, u32[]{:S(2)}) %collective-permute-start.4) | collective-permute-done | bytes 294944 | tf_op jit(solution)/shard_map/ppermute | solution.py:34
  23.8 0.0 collective-permute-start.5
  23.8 9.9 %expert.2 = (bf16[128,1024]{1,0:T(8,128)(2,1)S(1)}, bf16[128,1024]{1,0:T(8,128)(2,1)S(1)}, bf16[3072,2048]{1,0:T(8,128)(2,1)S(1)}) custom-call(bf16[128,1152]{1,0:T(8,128)(2,1)S(1)} %pad_maximum_fusion.refs_0_, bf16[128,1152]{1,0:T(8,128)(2,1)S(1)} %collective-permute-done.2.refs_1_, f32[1,2048]{1,0:T(1,128)} %bitcast.9, ...), custom_call_target="tpu_custom_call" | custom-call | flops 4831838208 | bytes 37748736 | tf_op jit(solution)/shard_map/expert/pallas_call | solution.py:163
  33.7 6.1 %expert.3 = (bf16[128,1024]{1,0:T(8,128)(2,1)S(1)}, bf16[128,1024]{1,0:T(8,128)(2,1)S(1)}) custom-call(bf16[128,1152]{1,0:T(8,128)(2,1)S(1)} %collective-permute-done.4.refs_0_, bf16[128,1152]{1,0:T(8,128)(2,1)S(1)} %collective-permute-done.5.refs_1_, f32[1,2048]{1,0:T(1,128)} %bitcast.10, bf16[2048,3072]{1,0:T(8,128)(2,1)S(1)} %fetch.2.refs_3_, ...), custom_call_target="tpu_custom_call" | custom-call | flops 4831838208 | bytes 37748736 | tf_op jit(solution)/shard_map/expert/pallas_call | solution.py:163
  39.9 0.6 collective-permute-start.6
  40.4 0.1 collective-permute-start.3
  40.5 1.1 %collective-permute-done.6 = bf16[128,1024]{1,0:T(8,128)(2,1)S(1)} collective-permute-done((bf16[128,1024]{1,0:T(8,128)(2,1)S(1)}, bf16[128,1024]{1,0:T(8,128)(2,1)S(1)}, u32[]{:S(2)}, u32[]{:S(2)}) %collective-permute-start.6) | collective-permute-done | bytes 262176 | tf_op jit(solution)/shard_map/ppermute | solution.py:34
  41.6 0.1 add_convert_fusion.1
  41.7 1.6 %collective-permute-start.7 = (bf16[128,1024]{1,0:T(8,128)(2,1)S(1)}, bf16[128,1024]{1,0:T(8,128)(2,1)S(1)}, u32[]{:S(2)}, u32[]{:S(2)}) collective-permute-start(bf16[128,1024]{1,0:T(8,128)(2,1)S(1)} %add_convert_fusion.1), channel_id=1, source_target_pairs={{0,2},{2,0},{4,6},{6,4},{8,10},{10,8},{12,14},{14,12},{1,3},{3,1},... | collective-permute-start | bytes 786440 | tf_op jit(solution)/shard_map/ppermute | solution.py:34
  43.3 7.0 %collective-permute-done.7 = bf16[128,1024]{1,0:T(8,128)(2,1)S(1)} collective-permute-done((bf16[128,1024]{1,0:T(8,128)(2,1)S(1)}, bf16[128,1024]{1,0:T(8,128)(2,1)S(1)}, u32[]{:S(2)}, u32[]{:S(2)}) %collective-permute-start.7) | collective-permute-done | bytes 262176 | tf_op jit(solution)/shard_map/ppermute | solution.py:34
  50.3 0.1 add_convert_fusion
  50.5 1.4 %collective-permute-start.8 = (bf16[64,1024]{1,0:T(8,128)(2,1)S(1)}, bf16[64,1024]{1,0:T(8,128)(2,1)S(1)}, u32[]{:S(2)}, u32[]{:S(2)}) collective-permute-start(bf16[64,1024]{1,0:T(8,128)(2,1)S(1)} %slice.17), channel_id=1, source_target_pairs={{0,4},{2,6},{4,0},{6,2},{8,12},{10,14},{12,8},{14,10},{1,5},{3,7},... | collective-permute-start | bytes 393224 | tf_op jit(solution)/shard_map/ppermute | solution.py:34
  51.9 3.6 %collective-permute-done.8 = bf16[64,1024]{1,0:T(8,128)(2,1)S(1)} collective-permute-done((bf16[64,1024]{1,0:T(8,128)(2,1)S(1)}, bf16[64,1024]{1,0:T(8,128)(2,1)S(1)}, u32[]{:S(2)}, u32[]{:S(2)}) %collective-permute-start.8) | collective-permute-done | bytes 131104 | tf_op jit(solution)/shard_map/ppermute | solution.py:34
  55.6 3.4 %collective-permute-start.9 = (bf16[32,1024]{1,0:T(8,128)(2,1)S(1)}, bf16[32,1024]{1,0:T(8,128)(2,1)S(1)}, u32[]{:S(2)}, u32[]{:S(2)}) collective-permute-start(bf16[32,1024]{1,0:T(8,128)(2,1)S(1)} %slice.19), channel_id=1, source_target_pairs={{0,8},{2,10},{4,12},{6,14},{8,0},{10,2},{12,4},{14,6},{1,9},{3,11}... | collective-permute-start | bytes 196616 | tf_op jit(solution)/shard_map/ppermute | solution.py:34
  59.0 2.9 %collective-permute-done.9 = bf16[32,1024]{1,0:T(8,128)(2,1)S(1)} collective-permute-done((bf16[32,1024]{1,0:T(8,128)(2,1)S(1)}, bf16[32,1024]{1,0:T(8,128)(2,1)S(1)}, u32[]{:S(2)}, u32[]{:S(2)}) %collective-permute-start.9) | collective-permute-done | bytes 65568 | tf_op jit(solution)/shard_map/ppermute | solution.py:34
  61.9 0.6 %add_convert_fusion.4 = bf16[32,1024]{1,0:T(8,128)(2,1)} fusion(bf16[32,1024]{1,0:T(8,128)(2,1)S(1)} %collective-permute-done.9, bf16[64,1024]{1,0:T(8,128)(2,1)S(1)} %add_convert_fusion.3), kind=kLoop, calls=%fused_computation.6 | loop fusion | flops 131072 | bytes 196608 | tf_op jit(solution)/shard_map/convert_element_type | solution.py:192
  (9 shorter events, 0.1 us)
Async XLA Ops:
  0.9 8.0 %collective-permute-start = (bf16[32,1152]{1,0:T(8,128)(2,1)S(1)}, bf16[32,1152]{1,0:T(8,128)(2,1)S(1)}, u32[]{:S(2)}, u32[]{:S(2)}) collective-permute-start(bf16[32,1152]{1,0:T(8,128)(2,1)S(1)} %prepare.1), channel_id=1, source_target_pairs={{0,8},{2,10},{4,12},{6,14},{8,0},{10,2},{12,4},{14,6},{1,9},{3,11}... | collective-permute-start | bytes 221192 | tf_op jit(solution)/shard_map/ppermute | solution.py:34
  9.0 5.3 %collective-permute-start.1 = (bf16[64,1152]{1,0:T(8,128)(2,1)S(1)}, bf16[64,1152]{1,0:T(8,128)(2,1)S(1)}, u32[]{:S(2)}, u32[]{:S(2)}) collective-permute-start(bf16[64,1152]{1,0:T(8,128)(2,1)S(1)} %pad_maximum_fusion.1), channel_id=1, source_target_pairs={{0,4},{2,6},{4,0},{6,2},{8,12},{10,14},{12,8},{14,10},{1,5},{3,7},... | collective-permute-start | bytes 442376 | tf_op jit(solution)/shard_map/ppermute | solution.py:34
  14.3 9.5 %collective-permute-start.2 = (bf16[128,1152]{1,0:T(8,128)(2,1)S(1)}, bf16[128,1152]{1,0:T(8,128)(2,1)S(1)}, u32[]{:S(2)}, u32[]{:S(2)}) collective-permute-start(bf16[128,1152]{1,0:T(8,128)(2,1)S(1)} %pad_maximum_fusion.refs_0_), channel_id=1, source_target_pairs={{0,1},{1,0},{2,3},{3,2},{4,5},{5,4},{6,7},{7,6},{8,9},{9,8},{10,11... | collective-permute-start | bytes 884744 | tf_op jit(solution)/shard_map/ppermute | solution.py:34
  14.4 9.4 %collective-permute-start.4 = (bf16[128,1152]{1,0:T(8,128)(2,1)S(1)}, bf16[128,1152]{1,0:T(8,128)(2,1)S(1)}, u32[]{:S(2)}, u32[]{:S(2)}) collective-permute-start(bf16[128,1152]{1,0:T(8,128)(2,1)S(1)} %pad_maximum_fusion.refs_0_), channel_id=1, source_target_pairs={{0,2},{2,0},{4,6},{6,4},{8,10},{10,8},{12,14},{14,12},{1,3},{3,1},... | collective-permute-start | bytes 884744 | tf_op jit(solution)/shard_map/ppermute | solution.py:34
  23.8 9.9 %collective-permute-start.5 = (bf16[128,1152]{1,0:T(8,128)(2,1)S(1)}, bf16[128,1152]{1,0:T(8,128)(2,1)S(1)}, u32[]{:S(2)}, u32[]{:S(2)}) collective-permute-start(bf16[128,1152]{1,0:T(8,128)(2,1)S(1)} %collective-permute-done.4.refs_0_), channel_id=1, source_target_pairs={{0,1},{1,0},{2,3},{3,2},{4,5},{5,4},{6,7},{7,6},{8,9},{9,8},{10,11... | collective-permute-start | bytes 884744 | tf_op jit(solution)/shard_map/ppermute | solution.py:34
  39.9 1.7 %collective-permute-start.6 = (bf16[128,1024]{1,0:T(8,128)(2,1)S(1)}, bf16[128,1024]{1,0:T(8,128)(2,1)S(1)}, u32[]{:S(2)}, u32[]{:S(2)}) collective-permute-start(bf16[128,1024]{1,0:T(8,128)(2,1)S(1)} %get-tuple-element.14), channel_id=1, source_target_pairs={{0,1},{1,0},{2,3},{3,2},{4,5},{5,4},{6,7},{7,6},{8,9},{9,8},{10,11... | collective-permute-start | bytes 786440 | tf_op jit(solution)/shard_map/ppermute | solution.py:34
  40.4 2.9 %collective-permute-start.3 = (bf16[128,1024]{1,0:T(8,128)(2,1)S(1)}, bf16[128,1024]{1,0:T(8,128)(2,1)S(1)}, u32[]{:S(2)}, u32[]{:S(2)}) collective-permute-start(bf16[128,1024]{1,0:T(8,128)(2,1)S(1)} %get-tuple-element.11), channel_id=1, source_target_pairs={{0,1},{1,0},{2,3},{3,2},{4,5},{5,4},{6,7},{7,6},{8,9},{9,8},{10,11... | collective-permute-start | bytes 786440 | tf_op jit(solution)/shard_map/ppermute | solution.py:34
  41.7 8.7 %collective-permute-start.7 = (bf16[128,1024]{1,0:T(8,128)(2,1)S(1)}, bf16[128,1024]{1,0:T(8,128)(2,1)S(1)}, u32[]{:S(2)}, u32[]{:S(2)}) collective-permute-start(bf16[128,1024]{1,0:T(8,128)(2,1)S(1)} %add_convert_fusion.1), channel_id=1, source_target_pairs={{0,2},{2,0},{4,6},{6,4},{8,10},{10,8},{12,14},{14,12},{1,3},{3,1},... | collective-permute-start | bytes 786440 | tf_op jit(solution)/shard_map/ppermute | solution.py:34
  50.5 5.0 %collective-permute-start.8 = (bf16[64,1024]{1,0:T(8,128)(2,1)S(1)}, bf16[64,1024]{1,0:T(8,128)(2,1)S(1)}, u32[]{:S(2)}, u32[]{:S(2)}) collective-permute-start(bf16[64,1024]{1,0:T(8,128)(2,1)S(1)} %slice.17), channel_id=1, source_target_pairs={{0,4},{2,6},{4,0},{6,2},{8,12},{10,14},{12,8},{14,10},{1,5},{3,7},... | collective-permute-start | bytes 393224 | tf_op jit(solution)/shard_map/ppermute | solution.py:34
  55.6 6.4 %collective-permute-start.9 = (bf16[32,1024]{1,0:T(8,128)(2,1)S(1)}, bf16[32,1024]{1,0:T(8,128)(2,1)S(1)}, u32[]{:S(2)}, u32[]{:S(2)}) collective-permute-start(bf16[32,1024]{1,0:T(8,128)(2,1)S(1)} %slice.19), channel_id=1, source_target_pairs={{0,8},{2,10},{4,12},{6,14},{8,0},{10,2},{12,4},{14,6},{1,9},{3,11}... | collective-permute-start | bytes 196616 | tf_op jit(solution)/shard_map/ppermute | solution.py:34

commit v2 on v1

v2 whole, which is shorter than its diff:
```python
import jax
import jax.numpy as jnp
from jax import lax
from jax.experimental import pallas as pl
from jax.experimental.pallas import tpu as pltpu
from jax.sharding import PartitionSpec as P


EPS = 1e-05
LANES = 128
MIB = 1 << 20


def vmem():
    return pl.BlockSpec(memory_space=pltpu.VMEM)


def hbm():
    return pl.BlockSpec(memory_space=pltpu.HBM)


def in_hbm(value):
    return pltpu.with_memory_space_constraint(value, pltpu.HBM)


def in_vmem(value):
    return pltpu.with_memory_space_constraint(value, pltpu.VMEM)


def cost(flops):
    return pl.CostEstimate(flops=flops, transcendentals=0, bytes_accessed=flops // 256)


def block_of(size, most):
    return max(b for b in range(LANES, most + 1, LANES) if size % b == 0)


def swap(value, axis, bit):
    return lax.ppermute(value, axis, [(i, i ^ bit) for i in range(lax.axis_size(axis))])


def prepare_body(tokens_hbm, routes_hbm, weights_hbm, out, tokens, routes, weights, sem):
    copies = [
        pltpu.make_async_copy(a, b, sem.at[i])
        for i, (a, b) in enumerate(
            ((routes_hbm, routes), (weights_hbm, weights), (tokens_hbm, tokens))
        )
    ]
    for copy in copies:
        copy.start()
    copies[0].wait()
    copies[1].wait()
    rows, width = tokens.shape
    lane = lax.broadcasted_iota(jnp.int32, (LANES, rows), 0)
    share = jnp.zeros((LANES, rows), jnp.float32)
    for k in range(routes.shape[0]):
        share = share + jnp.where(routes[k : k + 1, :] == lane, weights[k : k + 1, :], 0.0)
    out[:, width:] = share.T.astype(jnp.bfloat16)
    copies[2].wait()
    out[:, :width] = tokens[...]


def prepare(tokens, routes, weights):
    rows, width = tokens.shape
    arrays = (tokens, routes.T, weights.T)
    return pl.pallas_call(
        prepare_body,
        out_shape=jax.ShapeDtypeStruct((rows, width + LANES), jnp.bfloat16),
        in_specs=[hbm()] * 3,
        out_specs=vmem(),
        scratch_shapes=[pltpu.VMEM(a.shape, a.dtype) for a in arrays]
        + [pltpu.SemaphoreType.DMA((3,))],
        cost_estimate=cost(12 * 10**9),
        compiler_params=pltpu.CompilerParams(vmem_limit_bytes=2 * MIB),
        name="prepare",
    )(*(in_hbm(a) for a in arrays))


def half_at(far, width):
    core = lax.axis_index("tp")
    return pl.multiple_of((1 - core if far else core) * width, LANES)


def up_body(own, other, gain_hbm, w_gate, w_up, hidden, normed, gain, sem, *, width):
    gain_copy = pltpu.make_async_copy(gain_hbm, gain, sem)
    gain_copy.start()
    at = half_at(False, width)
    far = half_at(True, width)
    features = 2 * width
    mine = own[:, :width].astype(jnp.float32)
    theirs = other[:, :width].astype(jnp.float32)
    average = (
        jnp.sum(mine, axis=1, keepdims=True) + jnp.sum(theirs, axis=1, keepdims=True)
    ) / features
    mine = mine - average
    theirs = theirs - average
    spread = (
        jnp.sum(mine * mine, axis=1, keepdims=True)
        + jnp.sum(theirs * theirs, axis=1, keepdims=True)
    ) / features
    scale = lax.rsqrt(spread + EPS)
    gain_copy.wait()
    normed[:, pl.ds(at, width)] = (mine * scale * gain[:, pl.ds(at, width)]).astype(jnp.bfloat16)
    normed[:, pl.ds(far, width)] = (theirs * scale * gain[:, pl.ds(far, width)]).astype(
        jnp.bfloat16
    )
    chosen = normed[...]
    units = w_gate.shape[1]
    step = block_of(units, 512)
    for n in range(0, units, step):
        gate_val = jnp.dot(chosen, w_gate[:, n : n + step], preferred_element_type=jnp.float32)
        up_val = jnp.dot(chosen, w_up[:, n : n + step], preferred_element_type=jnp.float32)
        hidden[:, n : n + step] = (gate_val / (1.0 + jnp.exp(-gate_val)) * up_val).astype(
            jnp.bfloat16
        )


def project_up(own, other, gain, w_gate, w_up):
    rows, width = own.shape[0], own.shape[1] - LANES
    features, units = w_gate.shape
    return pl.pallas_call(
        lambda *refs: up_body(*refs, width=width),
        out_shape=jax.ShapeDtypeStruct((rows, units), jnp.bfloat16),
        in_specs=[vmem()] * 2 + [hbm()] + [vmem()] * 2,
        out_specs=vmem(),
        scratch_shapes=[
            pltpu.VMEM((rows, features), jnp.bfloat16),
            pltpu.VMEM((1, features), jnp.float32),
            pltpu.SemaphoreType.DMA,
        ],
        cost_estimate=cost(4 * rows * features * units),
        compiler_params=pltpu.CompilerParams(vmem_limit_bytes=8 * MIB),
        name="up",
    )(own, other, in_hbm(gain[None, :]), in_vmem(w_gate), in_vmem(w_up))


def down_body(own, hidden, w_down, out, *, far):
    width = out.shape[1]
    share = own[:, width:].astype(jnp.float32)
    lane = lax.broadcasted_iota(jnp.int32, share.shape, 1)
    share = jnp.sum(
        jnp.where(lane == lax.axis_index("ep"), share, 0.0), axis=1, keepdims=True
    )
    middle = hidden[...]
    step = block_of(width, 512)
    base = half_at(far, width)
    for n in range(0, width, step):
        part = jnp.dot(
            middle,
            w_down[:, pl.ds(pl.multiple_of(base + n, LANES), step)],
            preferred_element_type=jnp.float32,
        )
        out[:, n : n + step] = (part * share).astype(out.dtype)


def project_down(own, hidden, w_down, far):
    rows, units = hidden.shape
    width = own.shape[1] - LANES
    return pl.pallas_call(
        lambda *refs: down_body(*refs, far=far),
        out_shape=jax.ShapeDtypeStruct((rows, width), jnp.bfloat16),
        in_specs=[vmem()] * 3,
        out_specs=vmem(),
        cost_estimate=cost(2 * rows * units * width),
        compiler_params=pltpu.CompilerParams(vmem_limit_bytes=6 * MIB),
        name="down",
    )(own, hidden, in_vmem(w_down))


def add(*parts):
    return sum(p.astype(jnp.float32) for p in parts).astype(jnp.bfloat16)


def on_device_pair(tokens, gain, routes, weights, w_gate, w_up, w_down):
    return step_pair(tokens, gain, routes, weights, w_gate[0], w_up[0], w_down[0])


def step_pair(tokens, gain, routes, weights, w_gate, w_up, w_down):
    groups = lax.axis_size("ep")
    rows = tokens.shape[0]
    mine = prepare(tokens, routes, weights)
    column = sorted(range(2, groups, 2), key=lambda k: f"{k:b}"[::-1])
    near = [mine] + [swap(mine, "ep", k) for k in column]
    near = jnp.concatenate(near, axis=0)
    near_other = swap(near, "tp", 1)
    beside = swap(near, "ep", 1)
    near_hidden = project_up(near, near_other, gain, w_gate, w_up)
    near_send = project_down(near, near_hidden, w_down, True)
    near_back = swap(near_send, "tp", 1)
    beside_other = swap(beside, "tp", 1)
    near_keep = project_down(near, near_hidden, w_down, False)
    near_sum = add(near_keep, near_back)
    beside_hidden = project_up(beside, beside_other, gain, w_gate, w_up)
    beside_send = project_down(beside, beside_hidden, w_down, True)
    beside_back = swap(beside_send, "tp", 1)
    beside_keep = project_down(beside, beside_hidden, w_down, False)
    beside_sum = add(beside_keep, beside_back)
    bit = 1
    while near_sum.shape[0] > rows:
        half = near_sum.shape[0] // 2
        bit *= 2
        near_sum = add(near_sum[:half], swap(near_sum[half:], "ep", bit))
    parts = [near_sum]
    for i, k in enumerate([0] + column):
        block = beside_sum[i * rows : (i + 1) * rows]
        parts.append(swap(block, "ep", k + 1))
    return add(*parts)


def on_device_any(tokens, gain, routes, weights, w_gate, w_up, w_down):
    groups = lax.axis_size("ep")
    width = tokens.shape[1]
    rows = prepare(tokens, routes, weights)
    bits = [1 << i for i in reversed(range(groups.bit_length() - 1))]
    for bit in bits:
        rows = jnp.concatenate([rows, swap(rows, "ep", bit)], axis=0)
    lane = jnp.arange(LANES, dtype=jnp.int32)[None, :]
    share = jnp.where(lane == lax.axis_index("ep"), rows[:, width:].astype(jnp.float32), 0.0)
    share = jnp.sum(share, axis=1, keepdims=True)
    values = lax.all_gather(rows[:, :width], "tp", axis=1, tiled=True).astype(jnp.float32)
    values = values - jnp.mean(values, axis=1, keepdims=True)
    spread = jnp.mean(values * values, axis=1, keepdims=True)
    chosen = (values * lax.rsqrt(spread + EPS) * gain).astype(jnp.bfloat16)
    gate_val = jnp.dot(chosen, w_gate[0], preferred_element_type=jnp.float32)
    up_val = jnp.dot(chosen, w_up[0], preferred_element_type=jnp.float32)
    hidden = (jax.nn.silu(gate_val) * up_val).astype(jnp.bfloat16)
    part = jnp.dot(hidden, w_down[0], preferred_element_type=jnp.float32)
    total = lax.psum_scatter(
        (part * share).astype(jnp.bfloat16), "tp", scatter_dimension=1, tiled=True
    )
    for bit in reversed(bits):
        half = total.shape[0] // 2
        total = add(total[:half], swap(total[half:], "ep", bit))
    return total


def solution(mesh):
    in_specs = (
        P(("grp", "ep"), "tp"),
        P(),
        P(("grp", "ep"), None),
        P(("grp", "ep"), None),
        P("ep", None, "tp"),
        P("ep", None, "tp"),
        P("ep", "tp", None),
    )
    pair = mesh.shape["tp"] == 2 and mesh.shape["ep"] == 8
    return jax.shard_map(
        on_device_pair if pair else on_device_any,
        mesh=mesh,
        in_specs=in_specs,
        out_specs=P(("grp", "ep"), "tp"),
        check_vma=False,
    )
```

time: 62.9 us -> 45.7 us (0.73)
  Pallas kernels: 26.1 us -> 13.6 us
  waiting for transfers between devices: 21.7 us -> 14 us
  starting transfers between devices: 13.7 us -> 16.6 us
    pallas_call x4 -> x6, Pallas kernels: 25.2 us -> 12.6 us  [the longest x2 8.56 us: project_up(): pl.pallas_call(lambda *refs: up_body(*refs, width=width), out_shape=jax.S...]
    ppermute x10 -> x14, waiting for transfers between devices: 21.7 us -> 14 us  [swap(): lax.ppermute(value, axis, [(i, i ^ bit) for i in range(lax.axis_size(axis...]
    ppermute x10 -> x14, starting transfers between devices: 13.7 us -> 16.6 us  [swap(): lax.ppermute(value, axis, [(i, i ^ bit) for i in range(lax.axis_size(axis...]
  transfers between devices with their start and end apart: 10 -> 14, of which waited for: 6 -> 7; matrix products, arithmetic and copies ran while one was open for 0% -> 0% of each run, Pallas kernels for 30% -> 28%
where the time goes in v2:
time: 45.7 us; the launch traced here: 45.5 us
  starting transfers between devices  16.6 us (36%)
  waiting for transfers between devices  14 us (31%)
  Pallas kernels  13.6 us (30%)
  other arithmetic  0.88 us (2%)
    ppermute x14, starting transfers between devices, swap(): lax.ppermute(value, axis, [(i, i ^ bit) for i in range(lax.axis_size(axis...  16.6 us
    ppermute x14, waiting for transfers between devices, swap(): lax.ppermute(value, axis, [(i, i ^ bit) for i in range(lax.axis_size(axis...  14 us
    pallas_call x2, Pallas kernels, project_up(): pl.pallas_call(lambda *refs: up_body(*refs, width=width), out_shape=jax.S...  8.56 us
    pallas_call x4, Pallas kernels, project_down(): pl.pallas_call(lambda *refs: down_body(*refs, far=far), out_shape=jax.Sha...  4.01 us
    pallas_call x1, Pallas kernels, prepare(): pl.pallas_call(prepare_body, out_shape=jax.ShapeDtypeStruct((rows, width...  1.05 us
  transfers between devices with their start and end apart: 14, of which 7 were waited for; matrix products, arithmetic and copies ran while one was open for 0% of the time, Pallas kernels for 28%

profile of v2, /device:TPU:0, one launch (start us, length us, event | category | flops | bytes accessed | tf_op | source)
XLA Modules:
  0.0 45.5 jit_solution(14590374485762430647)
XLA Ops:
  0.0 1.1 %prepare.1 = bf16[32,1152]{1,0:T(8,128)(2,1)S(1)} custom-call(bf16[32,1024]{1,0:T(8,128)(2,1)} %tokens_hbm.1, s32[4,32]{1,0:T(4,128)} %bitcast.20, f32[4,32]{1,0:T(4,128)} %bitcast.21), custom_call_target="tpu_custom_call" | custom-call | flops 12000000000 | bytes 46875000 | tf_op jit(solution)/shard_map/prepare/pallas_call | solution.py:66
  1.1 4.1 %collective-permute-start = (bf16[32,1152]{1,0:T(8,128)(2,1)S(1)}, bf16[32,1152]{1,0:T(8,128)(2,1)S(1)}, u32[]{:S(2)}, u32[]{:S(2)}) collective-permute-start(bf16[32,1152]{1,0:T(8,128)(2,1)S(1)} %prepare.1), channel_id=1, source_target_pairs={{0,8},{2,10},{4,12},{6,14},{8,0},{10,2},{12,4},{14,6},{1,9},{3,11}... | collective-permute-start | bytes 221192 | tf_op jit(solution)/shard_map/ppermute | solution.py:39
  5.2 1.6 %collective-permute-start.1 = (bf16[32,1152]{1,0:T(8,128)(2,1)S(1)}, bf16[32,1152]{1,0:T(8,128)(2,1)S(1)}, u32[]{:S(2)}, u32[]{:S(2)}) collective-permute-start(bf16[32,1152]{1,0:T(8,128)(2,1)S(1)} %prepare.1), channel_id=1, source_target_pairs={{0,4},{2,6},{4,0},{6,2},{8,12},{10,14},{12,8},{14,10},{1,5},{3,7},... | collective-permute-start | bytes 221192 | tf_op jit(solution)/shard_map/ppermute | solution.py:39
  6.8 1.8 %collective-permute-done = bf16[32,1152]{1,0:T(8,128)(2,1)S(1)} collective-permute-done((bf16[32,1152]{1,0:T(8,128)(2,1)S(1)}, bf16[32,1152]{1,0:T(8,128)(2,1)S(1)}, u32[]{:S(2)}, u32[]{:S(2)}) %collective-permute-start) | collective-permute-done | bytes 73760 | tf_op jit(solution)/shard_map/ppermute | solution.py:39
  8.6 1.0 %collective-permute-done.1 = bf16[32,1152]{1,0:T(8,128)(2,1)S(1)} collective-permute-done((bf16[32,1152]{1,0:T(8,128)(2,1)S(1)}, bf16[32,1152]{1,0:T(8,128)(2,1)S(1)}, u32[]{:S(2)}, u32[]{:S(2)}) %collective-permute-start.1) | collective-permute-done | bytes 73760 | tf_op jit(solution)/shard_map/ppermute | solution.py:39
  9.6 3.4 %collective-permute-done.2 = bf16[32,1152]{1,0:T(8,128)(2,1)S(1)} collective-permute-done((bf16[32,1152]{1,0:T(8,128)(2,1)S(1)}, bf16[32,1152]{1,0:T(8,128)(2,1)S(1)}, u32[]{:S(2)}, u32[]{:S(2)}) %collective-permute-start.2) | collective-permute-done | bytes 73760 | tf_op jit(solution)/shard_map/ppermute | solution.py:39
  13.0 1.6 %collective-permute-start.7 = (bf16[128,1152]{1,0:T(8,128)(2,1)S(1)}, bf16[128,1152]{1,0:T(8,128)(2,1)S(1)}, u32[]{:S(2)}, u32[]{:S(2)}) collective-permute-start(bf16[128,1152]{1,0:T(8,128)(2,1)S(1)} %pad_maximum_fusion.refs_0_), channel_id=1, source_target_pairs={{0,2},{2,0},{4,6},{6,4},{8,10},{10,8},{12,14},{14,12},{1,3},{3,1},... | collective-permute-start | bytes 884744 | tf_op jit(solution)/shard_map/ppermute | solution.py:39
  14.6 4.4 %up.2.refs_1_ = bf16[128,3072]{1,0:T(8,128)(2,1)S(1)} custom-call(bf16[128,1152]{1,0:T(8,128)(2,1)S(1)} %pad_maximum_fusion.refs_0_, bf16[128,1152]{1,0:T(8,128)(2,1)S(1)} %collective-permute-done.3.refs_1_, f32[1,2048]{1,0:T(1,128)} %bitcast.18, bf16[2048,3072]{1,0:T(8,128)(2,1)S(1)} %bitcast.12, bf16[2048,3072]{1,0:T(8,128)(2,1)S(1)} %bitcast.14), custom_call_target="tpu_custom_call" | custom-call | flops 3221225472 | bytes 12582912 | tf_op jit(solution)/shard_map/up/pallas_call | solution.py:121
  19.1 1.0 %down.5 = bf16[128,1024]{1,0:T(8,128)(2,1)S(1)} custom-call(bf16[128,1152]{1,0:T(8,128)(2,1)S(1)} %pad_maximum_fusion.refs_0_, bf16[128,3072]{1,0:T(8,128)(2,1)S(1)} %up.2.refs_1_, bf16[3072,2048]{1,0:T(8,128)(2,1)S(1)} %bitcast.8), custom_call_target="tpu_custom_call" | custom-call | flops 805306368 | bytes 3145728 | tf_op jit(solution)/shard_map/down/pallas_call | solution.py:159
  20.1 0.2 collective-permute-start.4
  20.3 2.1 %collective-permute-done.7.refs_0_ = bf16[128,1152]{1,0:T(8,128)(2,1)S(1)} collective-permute-done((bf16[128,1152]{1,0:T(8,128)(2,1)S(1)}, bf16[128,1152]{1,0:T(8,128)(2,1)S(1)}, u32[]{:S(2)}, u32[]{:S(2)}) %collective-permute-start.7) | collective-permute-done | bytes 294944 | tf_op jit(solution)/shard_map/ppermute | solution.py:39
  22.5 1.0 %down.4 = bf16[128,1024]{1,0:T(8,128)(2,1)S(1)} custom-call(bf16[128,1152]{1,0:T(8,128)(2,1)S(1)} %pad_maximum_fusion.refs_0_, bf16[128,3072]{1,0:T(8,128)(2,1)S(1)} %up.2.refs_1_, bf16[3072,2048]{1,0:T(8,128)(2,1)S(1)} %bitcast.9), custom_call_target="tpu_custom_call" | custom-call | flops 805306368 | bytes 3145728 | tf_op jit(solution)/shard_map/down/pallas_call | solution.py:159
  23.7 0.4 collective-permute-done.8.refs_1_
  24.1 4.2 %up.3.refs_1_ = bf16[128,3072]{1,0:T(8,128)(2,1)S(1)} custom-call(bf16[128,1152]{1,0:T(8,128)(2,1)S(1)} %collective-permute-done.7.refs_0_, bf16[128,1152]{1,0:T(8,128)(2,1)S(1)} %collective-permute-done.8.refs_1_, f32[1,2048]{1,0:T(1,128)} %bitcast.19, bf16[2048,3072]{1,0:T(8,128)(2,1)S(1)} %bitcast.13, bf16[2048,3072]{1,0:T(8,128)(2,1)S(1)} %bitcast.17), custom_call_target="tpu_custom_call" | custom-call | flops 3221225472 | bytes 12582912 | tf_op jit(solution)/shard_map/up/pallas_call | solution.py:121
  28.3 1.0 %down.7 = bf16[128,1024]{1,0:T(8,128)(2,1)S(1)} custom-call(bf16[128,1152]{1,0:T(8,128)(2,1)S(1)} %collective-permute-done.7.refs_0_, bf16[128,3072]{1,0:T(8,128)(2,1)S(1)} %up.3.refs_1_, bf16[3072,2048]{1,0:T(8,128)(2,1)S(1)} %bitcast.10), custom_call_target="tpu_custom_call" | custom-call | flops 805306368 | bytes 3145728 | tf_op jit(solution)/shard_map/down/pallas_call | solution.py:159
  29.5 1.0 %down.6 = bf16[128,1024]{1,0:T(8,128)(2,1)S(1)} custom-call(bf16[128,1152]{1,0:T(8,128)(2,1)S(1)} %collective-permute-done.7.refs_0_, bf16[128,3072]{1,0:T(8,128)(2,1)S(1)} %up.3.refs_1_, bf16[3072,2048]{1,0:T(8,128)(2,1)S(1)} %bitcast.11), custom_call_target="tpu_custom_call" | custom-call | flops 805306368 | bytes 3145728 | tf_op jit(solution)/shard_map/down/pallas_call | solution.py:159
  30.5 2.0 %collective-permute-start.6 = (bf16[32,1024]{1,0:T(8,128)(2,1)S(1)}, bf16[32,1024]{1,0:T(8,128)(2,1)S(1)}, u32[]{:S(2)}, u32[]{:S(2)}) collective-permute-start(bf16[32,1024]{1,0:T(8,128)(2,1)S(1)} %slice.35), channel_id=1, source_target_pairs={{0,8},{2,10},{4,12},{6,14},{8,0},{10,2},{12,4},{14,6},{1,9},{3,11}... | collective-permute-start | bytes 196616 | tf_op jit(solution)/shard_map/ppermute | solution.py:39
  32.6 1.6 %collective-permute-start.10 = (bf16[32,1024]{1,0:T(8,128)(2,1)S(1)}, bf16[32,1024]{1,0:T(8,128)(2,1)S(1)}, u32[]{:S(2)}, u32[]{:S(2)}) collective-permute-start(bf16[32,1024]{1,0:T(8,128)(2,1)S(1)} %get-tuple-element.5), channel_id=1, source_target_pairs={{0,2},{2,0},{4,6},{6,4},{8,10},{10,8},{12,14},{14,12},{1,3},{3,1},... | collective-permute-start | bytes 196616 | tf_op jit(solution)/shard_map/ppermute | solution.py:39
  34.2 1.0 %collective-permute-start.11 = (bf16[32,1024]{1,0:T(8,128)(2,1)S(1)}, bf16[32,1024]{1,0:T(8,128)(2,1)S(1)}, u32[]{:S(2)}, u32[]{:S(2)}) collective-permute-start(bf16[32,1024]{1,0:T(8,128)(2,1)S(1)} %get-tuple-element.8), channel_id=1, source_target_pairs={{0,10},{2,8},{4,14},{6,12},{8,2},{10,0},{12,6},{14,4},{1,11},{3,9}... | collective-permute-start | bytes 196616 | tf_op jit(solution)/shard_map/ppermute | solution.py:39
  35.2 2.6 %collective-permute-start.12 = (bf16[32,1024]{1,0:T(8,128)(2,1)S(1)}, bf16[32,1024]{1,0:T(8,128)(2,1)S(1)}, u32[]{:S(2)}, u32[]{:S(2)}) collective-permute-start(bf16[32,1024]{1,0:T(8,128)(2,1)S(1)} %get-tuple-element.7), channel_id=1, source_target_pairs={{0,6},{2,4},{4,2},{6,0},{8,14},{10,12},{12,10},{14,8},{1,7},{3,5},... | collective-permute-start | bytes 196616 | tf_op jit(solution)/shard_map/ppermute | solution.py:39
  37.8 1.6 %collective-permute-start.13 = (bf16[32,1024]{1,0:T(8,128)(2,1)S(1)}, bf16[32,1024]{1,0:T(8,128)(2,1)S(1)}, u32[]{:S(2)}, u32[]{:S(2)}) collective-permute-start(bf16[32,1024]{1,0:T(8,128)(2,1)S(1)} %get-tuple-element.6), channel_id=1, source_target_pairs={{0,14},{2,12},{4,10},{6,8},{8,6},{10,4},{12,2},{14,0},{1,15},{3,13... | collective-permute-start | bytes 196616 | tf_op jit(solution)/shard_map/ppermute | solution.py:39
  39.5 2.7 %collective-permute-done.11 = bf16[32,1024]{1,0:T(8,128)(2,1)S(1)} collective-permute-done((bf16[32,1024]{1,0:T(8,128)(2,1)S(1)}, bf16[32,1024]{1,0:T(8,128)(2,1)S(1)}, u32[]{:S(2)}, u32[]{:S(2)}) %collective-permute-start.11) | collective-permute-done | bytes 65568 | tf_op jit(solution)/shard_map/ppermute | solution.py:39
  42.2 2.6 %collective-permute-done.13 = bf16[32,1024]{1,0:T(8,128)(2,1)S(1)} collective-permute-done((bf16[32,1024]{1,0:T(8,128)(2,1)S(1)}, bf16[32,1024]{1,0:T(8,128)(2,1)S(1)}, u32[]{:S(2)}, u32[]{:S(2)}) %collective-permute-start.13) | collective-permute-done | bytes 65568 | tf_op jit(solution)/shard_map/ppermute | solution.py:39
  44.8 0.7 %add_convert_fusion.3 = bf16[32,1024]{1,0:T(8,128)(2,1)} fusion(bf16[32,1024]{1,0:T(8,128)(2,1)S(1)} %collective-permute-done.13, bf16[32,1024]{1,0:T(8,128)(2,1)S(1)} %collective-permute-done.12, bf16[32,1024]{1,0:T(8,128)(2,1)S(1)} %collective-permute-done.11, bf16[32,1024]{1,0:T(8,128)(2,1)S(1)} %collective-permute-done.10, ...), kind=kLoop, calls=%fused_computation.4 | loop fusion | flops 458752 | bytes 458752 | tf_op jit(solution)/shard_map/convert_element_type | solution.py:171
  (37 shorter events, 0.7 us)
Async XLA Ops:
  0.0 14.6 %copy-start = (bf16[1,2048,3072]{2,1,0:T(8,128)(2,1)S(1)}, bf16[1,2048,3072]{2,1,0:T(8,128)(2,1)}, u32[]{:S(2)}) copy-start(bf16[1,2048,3072]{2,1,0:T(8,128)(2,1)} %param.11) | copy-start | bytes 37748740
  0.0 14.6 %copy-start.1 = (bf16[1,2048,3072]{2,1,0:T(8,128)(2,1)S(1)}, bf16[1,2048,3072]{2,1,0:T(8,128)(2,1)}, u32[]{:S(2)}) copy-start(bf16[1,2048,3072]{2,1,0:T(8,128)(2,1)} %param.12) | copy-start | bytes 37748740
  0.0 19.0 %slice-start = ((s8[12582912]{0:T(1024)(128)(4,1)}), s8[4194304]{0:T(1024)(128)(4,1)S(1)}, s32[]{:S(2)}) async-start(s8[12582912]{0:T(1024)(128)(4,1)} %bitcast.6), calls=%async_computation | async-start | bytes 8388608
  0.0 19.0 %slice-start.1 = ((s8[12582912]{0:T(1024)(128)(4,1)}), s8[4194304]{0:T(1024)(128)(4,1)S(1)}, s32[]{:S(2)}) async-start(s8[12582912]{0:T(1024)(128)(4,1)} %bitcast.6), calls=%async_computation.1 | async-start | bytes 8388608
  1.1 7.5 %collective-permute-start = (bf16[32,1152]{1,0:T(8,128)(2,1)S(1)}, bf16[32,1152]{1,0:T(8,128)(2,1)S(1)}, u32[]{:S(2)}, u32[]{:S(2)}) collective-permute-start(bf16[32,1152]{1,0:T(8,128)(2,1)S(1)} %prepare.1), channel_id=1, source_target_pairs={{0,8},{2,10},{4,12},{6,14},{8,0},{10,2},{12,4},{14,6},{1,9},{3,11}... | collective-permute-start | bytes 221192 | tf_op jit(solution)/shard_map/ppermute | solution.py:39
  5.2 4.4 %collective-permute-start.1 = (bf16[32,1152]{1,0:T(8,128)(2,1)S(1)}, bf16[32,1152]{1,0:T(8,128)(2,1)S(1)}, u32[]{:S(2)}, u32[]{:S(2)}) collective-permute-start(bf16[32,1152]{1,0:T(8,128)(2,1)S(1)} %prepare.1), channel_id=1, source_target_pairs={{0,4},{2,6},{4,0},{6,2},{8,12},{10,14},{12,8},{14,10},{1,5},{3,7},... | collective-permute-start | bytes 221192 | tf_op jit(solution)/shard_map/ppermute | solution.py:39
  6.8 6.2 %collective-permute-start.2 = (bf16[32,1152]{1,0:T(8,128)(2,1)S(1)}, bf16[32,1152]{1,0:T(8,128)(2,1)S(1)}, u32[]{:S(2)}, u32[]{:S(2)}) collective-permute-start(bf16[32,1152]{1,0:T(8,128)(2,1)S(1)} %prepare.1), channel_id=1, source_target_pairs={{0,12},{2,14},{4,8},{6,10},{8,4},{10,6},{12,0},{14,2},{1,13},{3,15... | collective-permute-start | bytes 221192 | tf_op jit(solution)/shard_map/ppermute | solution.py:39
  13.0 1.6 %collective-permute-start.3 = (bf16[128,1152]{1,0:T(8,128)(2,1)S(1)}, bf16[128,1152]{1,0:T(8,128)(2,1)S(1)}, u32[]{:S(2)}, u32[]{:S(2)}) collective-permute-start(bf16[128,1152]{1,0:T(8,128)(2,1)S(1)} %pad_maximum_fusion.refs_0_), channel_id=1, source_target_pairs={{0,1},{1,0},{2,3},{3,2},{4,5},{5,4},{6,7},{7,6},{8,9},{9,8},{10,11... | collective-permute-start | bytes 884744 | tf_op jit(solution)/shard_map/ppermute | solution.py:39
  13.0 9.4 %collective-permute-start.7 = (bf16[128,1152]{1,0:T(8,128)(2,1)S(1)}, bf16[128,1152]{1,0:T(8,128)(2,1)S(1)}, u32[]{:S(2)}, u32[]{:S(2)}) collective-permute-start(bf16[128,1152]{1,0:T(8,128)(2,1)S(1)} %pad_maximum_fusion.refs_0_), channel_id=1, source_target_pairs={{0,2},{2,0},{4,6},{6,4},{8,10},{10,8},{12,14},{14,12},{1,3},{3,1},... | collective-permute-start | bytes 884744 | tf_op jit(solution)/shard_map/ppermute | solution.py:39
  14.6 4.4 %slice-start.2 = ((s8[12582912]{0:T(1024)(128)(4,1)}), s8[4194304]{0:T(1024)(128)(4,1)S(1)}, s32[]{:S(2)}) async-start(s8[12582912]{0:T(1024)(128)(4,1)} %bitcast.6), calls=%async_computation.2 | async-start | bytes 8388608
  19.0 5.0 %slice-start.3 = ((s8[12582912]{0:T(1024)(128)(4,1)}), s8[4194304]{0:T(1024)(128)(4,1)S(1)}, s32[]{:S(2)}) async-start(s8[12582912]{0:T(1024)(128)(4,1)} %bitcast.15), calls=%async_computation.3 | async-start | bytes 8388608
  19.1 5.0 %slice-start.4 = ((s8[12582912]{0:T(1024)(128)(4,1)}), s8[4194304]{0:T(1024)(128)(4,1)S(1)}, s32[]{:S(2)}) async-start(s8[12582912]{0:T(1024)(128)(4,1)} %bitcast.15), calls=%async_computation.4 | async-start | bytes 8388608
  20.1 4.0 %slice-start.5 = ((s8[12582912]{0:T(1024)(128)(4,1)}), s8[4194304]{0:T(1024)(128)(4,1)S(1)}, s32[]{:S(2)}) async-start(s8[12582912]{0:T(1024)(128)(4,1)} %bitcast.15), calls=%async_computation.5 | async-start | bytes 8388608
  20.1 3.4 %collective-permute-start.4 = (bf16[128,1024]{1,0:T(8,128)(2,1)S(1)}, bf16[128,1024]{1,0:T(8,128)(2,1)S(1)}, u32[]{:S(2)}, u32[]{:S(2)}) collective-permute-start(bf16[128,1024]{1,0:T(8,128)(2,1)S(1)} %down.5), channel_id=1, source_target_pairs={{0,1},{1,0},{2,3},{3,2},{4,5},{5,4},{6,7},{7,6},{8,9},{9,8},{10,11... | collective-permute-start | bytes 786440 | tf_op jit(solution)/shard_map/ppermute | solution.py:39
  22.5 1.6 %collective-permute-start.8 = (bf16[128,1152]{1,0:T(8,128)(2,1)S(1)}, bf16[128,1152]{1,0:T(8,128)(2,1)S(1)}, u32[]{:S(2)}, u32[]{:S(2)}) collective-permute-start(bf16[128,1152]{1,0:T(8,128)(2,1)S(1)} %collective-permute-done.7.refs_0_), channel_id=1, source_target_pairs={{0,1},{1,0},{2,3},{3,2},{4,5},{5,4},{6,7},{7,6},{8,9},{9,8},{10,11... | collective-permute-start | bytes 884744 | tf_op jit(solution)/shard_map/ppermute | solution.py:39
  23.6 6.9 %collective-permute-start.5 = (bf16[64,1024]{1,0:T(8,128)(2,1)S(1)}, bf16[64,1024]{1,0:T(8,128)(2,1)S(1)}, u32[]{:S(2)}, u32[]{:S(2)}) collective-permute-start(bf16[64,1024]{1,0:T(8,128)(2,1)S(1)} %slice.33), channel_id=1, source_target_pairs={{0,4},{2,6},{4,0},{6,2},{8,12},{10,14},{12,8},{14,10},{1,5},{3,7},... | collective-permute-start | bytes 393224 | tf_op jit(solution)/shard_map/ppermute | solution.py:39
  29.3 3.3 %collective-permute-start.9 = (bf16[128,1024]{1,0:T(8,128)(2,1)S(1)}, bf16[128,1024]{1,0:T(8,128)(2,1)S(1)}, u32[]{:S(2)}, u32[]{:S(2)}) collective-permute-start(bf16[128,1024]{1,0:T(8,128)(2,1)S(1)} %down.7), channel_id=1, source_target_pairs={{0,1},{1,0},{2,3},{3,2},{4,5},{5,4},{6,7},{7,6},{8,9},{9,8},{10,11... | collective-permute-start | bytes 786440 | tf_op jit(solution)/shard_map/ppermute | solution.py:39
  30.5 8.9 %collective-permute-start.6 = (bf16[32,1024]{1,0:T(8,128)(2,1)S(1)}, bf16[32,1024]{1,0:T(8,128)(2,1)S(1)}, u32[]{:S(2)}, u32[]{:S(2)}) collective-permute-start(bf16[32,1024]{1,0:T(8,128)(2,1)S(1)} %slice.35), channel_id=1, source_target_pairs={{0,8},{2,10},{4,12},{6,14},{8,0},{10,2},{12,4},{14,6},{1,9},{3,11}... | collective-permute-start | bytes 196616 | tf_op jit(solution)/shard_map/ppermute | solution.py:39
  32.6 6.8 %collective-permute-start.10 = (bf16[32,1024]{1,0:T(8,128)(2,1)S(1)}, bf16[32,1024]{1,0:T(8,128)(2,1)S(1)}, u32[]{:S(2)}, u32[]{:S(2)}) collective-permute-start(bf16[32,1024]{1,0:T(8,128)(2,1)S(1)} %get-tuple-element.5), channel_id=1, source_target_pairs={{0,2},{2,0},{4,6},{6,4},{8,10},{10,8},{12,14},{14,12},{1,3},{3,1},... | collective-permute-start | bytes 196616 | tf_op jit(solution)/shard_map/ppermute | solution.py:39
  34.2 8.0 %collective-permute-start.11 = (bf16[32,1024]{1,0:T(8,128)(2,1)S(1)}, bf16[32,1024]{1,0:T(8,128)(2,1)S(1)}, u32[]{:S(2)}, u32[]{:S(2)}) collective-permute-start(bf16[32,1024]{1,0:T(8,128)(2,1)S(1)} %get-tuple-element.8), channel_id=1, source_target_pairs={{0,10},{2,8},{4,14},{6,12},{8,2},{10,0},{12,6},{14,4},{1,11},{3,9}... | collective-permute-start | bytes 196616 | tf_op jit(solution)/shard_map/ppermute | solution.py:39
  35.2 7.0 %collective-permute-start.12 = (bf16[32,1024]{1,0:T(8,128)(2,1)S(1)}, bf16[32,1024]{1,0:T(8,128)(2,1)S(1)}, u32[]{:S(2)}, u32[]{:S(2)}) collective-permute-start(bf16[32,1024]{1,0:T(8,128)(2,1)S(1)} %get-tuple-element.7), channel_id=1, source_target_pairs={{0,6},{2,4},{4,2},{6,0},{8,14},{10,12},{12,10},{14,8},{1,7},{3,5},... | collective-permute-start | bytes 196616 | tf_op jit(solution)/shard_map/ppermute | solution.py:39
  37.8 7.0 %collective-permute-start.13 = (bf16[32,1024]{1,0:T(8,128)(2,1)S(1)}, bf16[32,1024]{1,0:T(8,128)(2,1)S(1)}, u32[]{:S(2)}, u32[]{:S(2)}) collective-permute-start(bf16[32,1024]{1,0:T(8,128)(2,1)S(1)} %get-tuple-element.6), channel_id=1, source_target_pairs={{0,14},{2,12},{4,10},{6,8},{8,6},{10,4},{12,2},{14,0},{1,15},{3,13... | collective-permute-start | bytes 196616 | tf_op jit(solution)/shard_map/ppermute | solution.py:39

commit v3 on v2

--- a/solution.py
+++ b/solution.py
@@ -39,41 +39,50 @@
     return lax.ppermute(value, axis, [(i, i ^ bit) for i in range(lax.axis_size(axis))])
 
 
-def prepare_body(tokens_hbm, routes_hbm, weights_hbm, out, tokens, routes, weights, sem):
+def share_body(routes_hbm, weights_hbm, out, routes, weights, sem):
     copies = [
-        pltpu.make_async_copy(a, b, sem.at[i])
-        for i, (a, b) in enumerate(
-            ((routes_hbm, routes), (weights_hbm, weights), (tokens_hbm, tokens))
-        )
+        pltpu.make_async_copy(routes_hbm, routes, sem.at[0]),
+        pltpu.make_async_copy(weights_hbm, weights, sem.at[1]),
     ]
     for copy in copies:
         copy.start()
-    copies[0].wait()
-    copies[1].wait()
-    rows, width = tokens.shape
-    lane = lax.broadcasted_iota(jnp.int32, (LANES, rows), 0)
+    for copy in copies:
+        copy.wait()
+    top, rows = routes.shape
+    expert = lax.broadcasted_iota(jnp.int32, (LANES, rows), 0) ^ lax.axis_index("ep")
     share = jnp.zeros((LANES, rows), jnp.float32)
-    for k in range(routes.shape[0]):
-        share = share + jnp.where(routes[k : k + 1, :] == lane, weights[k : k + 1, :], 0.0)
-    out[:, width:] = share.T.astype(jnp.bfloat16)
-    copies[2].wait()
-    out[:, :width] = tokens[...]
-
-
-def prepare(tokens, routes, weights):
-    rows, width = tokens.shape
-    arrays = (tokens, routes.T, weights.T)
-    return pl.pallas_call(
-        prepare_body,
-        out_shape=jax.ShapeDtypeStruct((rows, width + LANES), jnp.bfloat16),
-        in_specs=[hbm()] * 3,
+    for k in range(top):
+        share = share + jnp.where(routes[k : k + 1, :] == expert, weights[k : k + 1, :], 0.0)
+    out[...] = share.T
+
+
+def shares(routes, weights):
+    arrays = (routes.T, weights.T)
+    return pl.pallas_call(
+        share_body,
+        out_shape=jax.ShapeDtypeStruct((routes.shape[0], LANES), jnp.float32),
+        in_specs=[hbm()] * 2,
         out_specs=vmem(),
         scratch_shapes=[pltpu.VMEM(a.shape, a.dtype) for a in arrays]
-        + [pltpu.SemaphoreType.DMA((3,))],
+        + [pltpu.SemaphoreType.DMA((2,))],
+        compiler_params=pltpu.CompilerParams(vmem_limit_bytes=2 * MIB),
+        name="shares",
+    )(*(in_hbm(a) for a in arrays))
+
+
+def open_body(out):
+    out[...] = jnp.zeros(out.shape, out.dtype)
+
+
+def opening():
+    return pl.pallas_call(
+        open_body,
+        out_shape=jax.ShapeDtypeStruct((8, LANES), jnp.float32),
+        out_specs=vmem(),
         cost_estimate=cost(12 * 10**9),
-        compiler_params=pltpu.CompilerParams(vmem_limit_bytes=2 * MIB),
-        name="prepare",
-    )(*(in_hbm(a) for a in arrays))
+        compiler_params=pltpu.CompilerParams(vmem_limit_bytes=MIB),
+        name="opening",
+    )()
 
 
 def half_at(far, width):
@@ -116,7 +125,7 @@
 
 
 def project_up(own, other, gain, w_gate, w_up):
-    rows, width = own.shape[0], own.shape[1] - LANES
+    rows, width = own.shape
     features, units = w_gate.shape
     return pl.pallas_call(
         lambda *refs: up_body(*refs, width=width),
@@ -134,13 +143,8 @@
     )(own, other, in_hbm(gain[None, :]), in_vmem(w_gate), in_vmem(w_up))
 
 
-def down_body(own, hidden, w_down, out, *, far):
+def down_body(hidden, w_down, out, *, far):
     width = out.shape[1]
-    share = own[:, width:].astype(jnp.float32)
-    lane = lax.broadcasted_iota(jnp.int32, share.shape, 1)
-    share = jnp.sum(
-        jnp.where(lane == lax.axis_index("ep"), share, 0.0), axis=1, keepdims=True
-    )
     middle = hidden[...]
     step = block_of(width, 512)
     base = half_at(far, width)
@@ -150,21 +154,62 @@
             w_down[:, pl.ds(pl.multiple_of(base + n, LANES), step)],
             preferred_element_type=jnp.float32,
         )
-        out[:, n : n + step] = (part * share).astype(out.dtype)
-
-
-def project_down(own, hidden, w_down, far):
+        out[:, n : n + step] = part.astype(out.dtype)
+
+
+def project_down(hidden, w_down, far):
     rows, units = hidden.shape
-    width = own.shape[1] - LANES
+    width = w_down.shape[1] // 2
     return pl.pallas_call(
         lambda *refs: down_body(*refs, far=far),
         out_shape=jax.ShapeDtypeStruct((rows, width), jnp.bfloat16),
-        in_specs=[vmem()] * 3,
+        in_specs=[vmem()] * 2,
         out_specs=vmem(),
         cost_estimate=cost(2 * rows * units * width),
         compiler_params=pltpu.CompilerParams(vmem_limit_bytes=6 * MIB),
         name="down",
-    )(own, hidden, in_vmem(w_down))
+    )(hidden, in_vmem(w_down))
+
+
+def combine_body(zero, share, order, *refs):
+    blocks, out, total, sem = refs[:-3], refs[-3], refs[-2], refs[-1]
+    rows, width = total.shape
+    copies = []
+    step = block_of(width, 512)
+    for n in range(0, width, step):
+        part = jnp.tile(zero[...], (rows // 8, step // LANES))
+        for k, block in zip(order, blocks):
+            weight = share[:, k : k + 1]
+            part = part + block[:rows, n : n + step].astype(jnp.float32) * weight
+        total[:, n : n + step] = part.astype(total.dtype)
+        copies.append(
+            pltpu.make_async_copy(
+                total.at[:, n : n + step], out.at[:, n : n + step], sem.at[n // step]
+            )
+        )
+        copies[-1].start()
+    for copy in copies:
+        copy.wait()
+
+
+def combine(zero, share, blocks):
+    rows = share.shape[0]
+    width = blocks[0][1].shape[1]
+    order = [k for k, _ in blocks]
+    values = [value for _, value in blocks]
+    body = lambda zero, share, *refs: combine_body(zero, share, order, *refs)
+    return pl.pallas_call(
+        body,
+        out_shape=jax.ShapeDtypeStruct((rows, width), jnp.bfloat16),
+        in_specs=[vmem()] * (2 + len(values)),
+        out_specs=hbm(),
+        scratch_shapes=[
+            pltpu.VMEM((rows, width), jnp.bfloat16),
+            pltpu.SemaphoreType.DMA((width // block_of(width, 512),)),
+        ],
+        compiler_params=pltpu.CompilerParams(vmem_limit_bytes=2 * MIB),
+        name="combine",
+    )(zero, share, *values)
 
 
 def add(*parts):
@@ -178,44 +223,43 @@
 def step_pair(tokens, gain, routes, weights, w_gate, w_up, w_down):
     groups = lax.axis_size("ep")
     rows = tokens.shape[0]
-    mine = prepare(tokens, routes, weights)
-    column = sorted(range(2, groups, 2), key=lambda k: f"{k:b}"[::-1])
-    near = [mine] + [swap(mine, "ep", k) for k in column]
+    zero = opening()
+    share = shares(routes, weights)
+    column = range(2, groups, 2)
+    near = [tokens] + [swap(tokens, "ep", k) for k in column]
     near = jnp.concatenate(near, axis=0)
     near_other = swap(near, "tp", 1)
     beside = swap(near, "ep", 1)
     near_hidden = project_up(near, near_other, gain, w_gate, w_up)
-    near_send = project_down(near, near_hidden, w_down, True)
+    near_send = project_down(near_hidden, w_down, True)
     near_back = swap(near_send, "tp", 1)
     beside_other = swap(beside, "tp", 1)
-    near_keep = project_down(near, near_hidden, w_down, False)
+    near_keep = project_down(near_hidden, w_down, False)
     near_sum = add(near_keep, near_back)
     beside_hidden = project_up(beside, beside_other, gain, w_gate, w_up)
-    beside_send = project_down(beside, beside_hidden, w_down, True)
+    beside_send = project_down(beside_hidden, w_down, True)
     beside_back = swap(beside_send, "tp", 1)
-    beside_keep = project_down(beside, beside_hidden, w_down, False)
+    beside_keep = project_down(beside_hidden, w_down, False)
     beside_sum = add(beside_keep, beside_back)
-    bit = 1
-    while near_sum.shape[0] > rows:
-        half = near_sum.shape[0] // 2
-        bit *= 2
-        near_sum = add(near_sum[:half], swap(near_sum[half:], "ep", bit))
-    parts = [near_sum]
-    for i, k in enumerate([0] + column):
-        block = beside_sum[i * rows : (i + 1) * rows]
-        parts.append(swap(block, "ep", k + 1))
-    return add(*parts)
+    blocks = []
+    for first, result in ((0, near_sum), (1, beside_sum)):
+        for i in range(groups // 2):
+            k = 2 * i + first
+            block = result[i * rows : (i + 1) * rows]
+            blocks.append((k, swap(block, "ep", k) if k else result))
+    return combine(zero, share, blocks)
 
 
 def on_device_any(tokens, gain, routes, weights, w_gate, w_up, w_down):
     groups = lax.axis_size("ep")
     width = tokens.shape[1]
-    rows = prepare(tokens, routes, weights)
+    experts = jnp.arange(LANES, dtype=jnp.int32)
+    share = jnp.where(routes[:, :, None] == experts, weights[:, :, None], 0.0).sum(axis=1)
+    rows = jnp.concatenate([tokens, share.astype(jnp.bfloat16)], axis=1)
     bits = [1 << i for i in reversed(range(groups.bit_length() - 1))]
     for bit in bits:
         rows = jnp.concatenate([rows, swap(rows, "ep", bit)], axis=0)
-    lane = jnp.arange(LANES, dtype=jnp.int32)[None, :]
-    share = jnp.where(lane == lax.axis_index("ep"), rows[:, width:].astype(jnp.float32), 0.0)
+    share = jnp.where(experts == lax.axis_index("ep"), rows[:, width:].astype(jnp.float32), 0.0)
     share = jnp.sum(share, axis=1, keepdims=True)
     values = lax.all_gather(rows[:, :width], "tp", axis=1, tiled=True).astype(jnp.float32)
     values = values - jnp.mean(values, axis=1, keepdims=True)

time: 45.7 us -> 64.8 us (1.42)
  local copies, waits for them, and re-layouts: 0.08 us -> 15.9 us
  starting transfers between devices: 16.6 us -> 19.5 us
  other arithmetic: 0.88 us -> 0.14 us
    unnamed x16 -> x21, local copies, waits for them, and re-layouts: 0.04 us -> 15.9 us
    ppermute x14 -> x15, starting transfers between devices: 16.6 us -> 19.5 us  [swap(): lax.ppermute(value, axis, [(i, i ^ bit) for i in range(lax.axis_size(axis...]
    convert_element_type x4 -> x2, other arithmetic: 0.86 us -> 0.13 us  [add(): return sum((p.astype(jnp.float32) for p in parts)).astype(jnp.bfloat16)]
    pallas_call x1 -> x3, Pallas kernels: 1.05 us -> 1.62 us  [the longest x1 0.82 us: combine(): pl.pallas_call(body, out_shape=jax.ShapeDtypeStruct((rows, width), jnp.bf...]
    ppermute x14 -> x15, waiting for transfers between devices: 14 us -> 14.4 us  [swap(): lax.ppermute(value, axis, [(i, i ^ bit) for i in range(lax.axis_size(axis...]
  transfers between devices with their start and end apart: 14 -> 15, of which waited for: 7 -> 5; matrix products, arithmetic and copies ran while one was open for 0% -> 2% of each run, Pallas kernels for 28% -> 21%
where the time goes in v3:
time: 64.8 us; the launch traced here: 64.5 us
  starting transfers between devices  19.5 us (30%)
  local copies, waits for them, and re-layouts  15.9 us (25%)
  waiting for transfers between devices  14.4 us (22%)
  Pallas kernels  14.2 us (22%)
    ppermute x15, starting transfers between devices, swap(): lax.ppermute(value, axis, [(i, i ^ bit) for i in range(lax.axis_size(axis...  19.5 us
    unnamed x21, local copies, waits for them, and re-layouts  15.9 us
    ppermute x15, waiting for transfers between devices, swap(): lax.ppermute(value, axis, [(i, i ^ bit) for i in range(lax.axis_size(axis...  14.4 us
    pallas_call x2, Pallas kernels, project_up(): pl.pallas_call(lambda *refs: up_body(*refs, width=width), out_shape=jax.S...  8.51 us
    pallas_call x4, Pallas kernels, project_down(): pl.pallas_call(lambda *refs: down_body(*refs, far=far), out_shape=jax.Sha...  4.05 us
  transfers between devices with their start and end apart: 15, of which 5 were waited for; matrix products, arithmetic and copies ran while one was open for 2% of the time, Pallas kernels for 21%

profile of v3, /device:TPU:0, one launch (start us, length us, event | category | flops | bytes accessed | tf_op | source)
XLA Modules:
  0.0 64.5 jit_solution(714671035774584283)
XLA Ops:
  0.0 3.1 %collective-permute-start = (bf16[32,1024]{1,0:T(8,128)(2,1)}, bf16[32,1024]{1,0:T(8,128)(2,1)S(1)}, u32[]{:S(2)}, u32[]{:S(2)}) collective-permute-start(bf16[32,1024]{1,0:T(8,128)(2,1)} %param.7), channel_id=1, source_target_pairs={{0,4},{2,6},{4,0},{6,2},{8,12},{10,14},{12,8},{14,10},{1,5},{3,7},... | collective-permute-start | bytes 196616 | tf_op jit(solution)/shard_map/ppermute | solution.py:39
  3.1 2.6 %collective-permute-start.1 = (bf16[32,1024]{1,0:T(8,128)(2,1)}, bf16[32,1024]{1,0:T(8,128)(2,1)S(1)}, u32[]{:S(2)}, u32[]{:S(2)}) collective-permute-start(bf16[32,1024]{1,0:T(8,128)(2,1)} %param.7), channel_id=1, source_target_pairs={{0,8},{2,10},{4,12},{6,14},{8,0},{10,2},{12,4},{14,6},{1,9},{3,11}... | collective-permute-start | bytes 196616 | tf_op jit(solution)/shard_map/ppermute | solution.py:39
  5.6 0.9 %constant_dynamic-update-slice_fusion.3 = bf16[128,1024]{1,0:T(8,128)(2,1)S(1)} fusion(bf16[32,1024]{1,0:T(8,128)(2,1)} %param.7), kind=kLoop, calls=%fused_computation.5 | loop fusion | bytes 131072
  6.6 4.0 %collective-permute-done.1 = bf16[32,1024]{1,0:T(8,128)(2,1)S(1)} collective-permute-done((bf16[32,1024]{1,0:T(8,128)(2,1)}, bf16[32,1024]{1,0:T(8,128)(2,1)S(1)}, u32[]{:S(2)}, u32[]{:S(2)}) %collective-permute-start.1) | collective-permute-done | bytes 65568 | tf_op jit(solution)/shard_map/ppermute | solution.py:39
  10.5 1.4 %collective-permute-done.2 = bf16[32,1024]{1,0:T(8,128)(2,1)S(1)} collective-permute-done((bf16[32,1024]{1,0:T(8,128)(2,1)}, bf16[32,1024]{1,0:T(8,128)(2,1)S(1)}, u32[]{:S(2)}, u32[]{:S(2)}) %collective-permute-start.2) | collective-permute-done | bytes 65568 | tf_op jit(solution)/shard_map/ppermute | solution.py:39
  12.0 1.5 %collective-permute-start.8 = (bf16[128,1024]{1,0:T(8,128)(2,1)S(1)}, bf16[128,1024]{1,0:T(8,128)(2,1)S(1)}, u32[]{:S(2)}, u32[]{:S(2)}) collective-permute-start(bf16[128,1024]{1,0:T(8,128)(2,1)S(1)} %constant_dynamic-update-slice_fusion.refs_0_), channel_id=1, source_target_pairs={{0,2},{2,0},{4,6},{6,4},{8,10},{10,8},{12,14},{14,12},{1,3},{3,1},... | collective-permute-start | bytes 786440 | tf_op jit(solution)/shard_map/ppermute | solution.py:39
  13.4 4.9 %collective-permute-done.8.refs_0_ = bf16[128,1024]{1,0:T(8,128)(2,1)S(1)} collective-permute-done((bf16[128,1024]{1,0:T(8,128)(2,1)S(1)}, bf16[128,1024]{1,0:T(8,128)(2,1)S(1)}, u32[]{:S(2)}, u32[]{:S(2)}) %collective-permute-start.8) | collective-permute-done | bytes 262176 | tf_op jit(solution)/shard_map/ppermute | solution.py:39
  18.4 4.6 %copy-done = bf16[1,2048,3072]{2,1,0:T(8,128)(2,1)S(1)} copy-done((bf16[1,2048,3072]{2,1,0:T(8,128)(2,1)S(1)}, bf16[1,2048,3072]{2,1,0:T(8,128)(2,1)}, u32[]{:S(2)}) %copy-start) | copy-done | bytes 12582936
  22.9 4.6 %copy-done.1 = bf16[1,2048,3072]{2,1,0:T(8,128)(2,1)S(1)} copy-done((bf16[1,2048,3072]{2,1,0:T(8,128)(2,1)S(1)}, bf16[1,2048,3072]{2,1,0:T(8,128)(2,1)}, u32[]{:S(2)}) %copy-start.1) | copy-done | bytes 12582936
  27.5 4.3 %up.2.refs_0_ = bf16[128,3072]{1,0:T(8,128)(2,1)S(1)} custom-call(bf16[128,1024]{1,0:T(8,128)(2,1)S(1)} %constant_dynamic-update-slice_fusion.refs_0_, bf16[128,1024]{1,0:T(8,128)(2,1)S(1)} %collective-permute-done.3.refs_1_, f32[1,2048]{1,0:T(1,128)} %bitcast.18, bf16[2048,3072]{1,0:T(8,128)(2,1)S(1)} %bitcast.12, bf16[2048,3072]{1,0:T(8,128)(2,1)S(1)} %bitcast.16), custom_call_target="tpu_custom_call" | custom-call | flops 3221225472 | bytes 12582912 | tf_op jit(solution)/shard_map/up/pallas_call | solution.py:130
  31.9 1.0 %down.5 = bf16[128,1024]{1,0:T(8,128)(2,1)S(1)} custom-call(bf16[128,3072]{1,0:T(8,128)(2,1)S(1)} %up.2.refs_0_, bf16[3072,2048]{1,0:T(8,128)(2,1)S(1)} %bitcast.8), custom_call_target="tpu_custom_call" | custom-call | flops 805306368 | bytes 3145728 | tf_op jit(solution)/shard_map/down/pallas_call | solution.py:163
  33.5 1.0 %down.4 = bf16[128,1024]{1,0:T(8,128)(2,1)S(1)} custom-call(bf16[128,3072]{1,0:T(8,128)(2,1)S(1)} %up.2.refs_0_, bf16[3072,2048]{1,0:T(8,128)(2,1)S(1)} %bitcast.9), custom_call_target="tpu_custom_call" | custom-call | flops 805306368 | bytes 3145728 | tf_op jit(solution)/shard_map/down/pallas_call | solution.py:163
  35.4 3.7 %copy-done.2 = bf16[1,2048,3072]{2,1,0:T(8,128)(2,1)S(1)} copy-done((bf16[1,2048,3072]{2,1,0:T(8,128)(2,1)S(1)}, bf16[1,2048,3072]{2,1,0:T(8,128)(2,1)}, u32[]{:S(2)}) %copy-start.2) | copy-done | bytes 12582936
  39.1 1.3 %slice-done.5 = s8[4194304]{0:T(1024)(128)(4,1)S(1)} async-done(((s8[12582912]{0:T(1024)(128)(4,1)}), s8[4194304]{0:T(1024)(128)(4,1)S(1)}, s32[]{:S(2)}) %slice-start.5) | async-done | bytes 4194328
  40.4 4.2 %up.3.refs_0_ = bf16[128,3072]{1,0:T(8,128)(2,1)S(1)} custom-call(bf16[128,1024]{1,0:T(8,128)(2,1)S(1)} %collective-permute-done.8.refs_0_, bf16[128,1024]{1,0:T(8,128)(2,1)S(1)} %collective-permute-done.9.refs_1_, f32[1,2048]{1,0:T(1,128)} %bitcast.19, bf16[2048,3072]{1,0:T(8,128)(2,1)S(1)} %bitcast.15, bf16[2048,3072]{1,0:T(8,128)(2,1)S(1)} %bitcast.17), custom_call_target="tpu_custom_call" | custom-call | flops 3221225472 | bytes 12582912 | tf_op jit(solution)/shard_map/up/pallas_call | solution.py:130
  44.6 1.0 %down.7 = bf16[128,1024]{1,0:T(8,128)(2,1)S(1)} custom-call(bf16[128,3072]{1,0:T(8,128)(2,1)S(1)} %up.3.refs_0_, bf16[3072,2048]{1,0:T(8,128)(2,1)S(1)} %bitcast.10), custom_call_target="tpu_custom_call" | custom-call | flops 805306368 | bytes 3145728 | tf_op jit(solution)/shard_map/down/pallas_call | solution.py:163
  47.1 1.6 %collective-permute-start.6 = (bf16[32,1024]{1,0:T(8,128)(2,1)S(1)}, bf16[32,1024]{1,0:T(8,128)(2,1)S(1)}, u32[]{:S(2)}, u32[]{:S(2)}) collective-permute-start(bf16[32,1024]{1,0:T(8,128)(2,1)S(1)} %get-tuple-element.10), channel_id=1, source_target_pairs={{0,8},{2,10},{4,12},{6,14},{8,0},{10,2},{12,4},{14,6},{1,9},{3,11}... | collective-permute-start | bytes 196616 | tf_op jit(solution)/shard_map/ppermute | solution.py:39
  48.7 2.0 %collective-permute-start.7 = (bf16[32,1024]{1,0:T(8,128)(2,1)S(1)}, bf16[32,1024]{1,0:T(8,128)(2,1)S(1)}, u32[]{:S(2)}, u32[]{:S(2)}) collective-permute-start(bf16[32,1024]{1,0:T(8,128)(2,1)S(1)} %get-tuple-element.9), channel_id=1, source_target_pairs={{0,12},{2,14},{4,8},{6,10},{8,4},{10,6},{12,0},{14,2},{1,13},{3,15... | collective-permute-start | bytes 196616 | tf_op jit(solution)/shard_map/ppermute | solution.py:39
  50.7 1.0 %down.6 = bf16[128,1024]{1,0:T(8,128)(2,1)S(1)} custom-call(bf16[128,3072]{1,0:T(8,128)(2,1)S(1)} %up.3.refs_0_, bf16[3072,2048]{1,0:T(8,128)(2,1)S(1)} %bitcast.11), custom_call_target="tpu_custom_call" | custom-call | flops 805306368 | bytes 3145728 | tf_op jit(solution)/shard_map/down/pallas_call | solution.py:163
  51.8 1.6 %collective-permute-start.11 = (bf16[32,1024]{1,0:T(8,128)(2,1)S(1)}, bf16[32,1024]{1,0:T(8,128)(2,1)S(1)}, u32[]{:S(2)}, u32[]{:S(2)}) collective-permute-start(bf16[32,1024]{1,0:T(8,128)(2,1)S(1)} %get-tuple-element.8), channel_id=1, source_target_pairs={{0,2},{2,0},{4,6},{6,4},{8,10},{10,8},{12,14},{14,12},{1,3},{3,1},... | collective-permute-start | bytes 196616 | tf_op jit(solution)/shard_map/ppermute | solution.py:39
  53.4 3.3 %collective-permute-start.13 = (bf16[32,1024]{1,0:T(8,128)(2,1)S(1)}, bf16[32,1024]{1,0:T(8,128)(2,1)S(1)}, u32[]{:S(2)}, u32[]{:S(2)}) collective-permute-start(bf16[32,1024]{1,0:T(8,128)(2,1)S(1)} %get-tuple-element.6), channel_id=1, source_target_pairs={{0,10},{2,8},{4,14},{6,12},{8,2},{10,0},{12,6},{14,4},{1,11},{3,9}... | collective-permute-start | bytes 196616 | tf_op jit(solution)/shard_map/ppermute | solution.py:39
  56.7 2.0 %collective-permute-start.14 = (bf16[32,1024]{1,0:T(8,128)(2,1)S(1)}, bf16[32,1024]{1,0:T(8,128)(2,1)S(1)}, u32[]{:S(2)}, u32[]{:S(2)}) collective-permute-start(bf16[32,1024]{1,0:T(8,128)(2,1)S(1)} %get-tuple-element.5), channel_id=1, source_target_pairs={{0,14},{2,12},{4,10},{6,8},{8,6},{10,4},{12,2},{14,0},{1,15},{3,13... | collective-permute-start | bytes 196616 | tf_op jit(solution)/shard_map/ppermute | solution.py:39
  60.2 3.5 %collective-permute-done.14.refs_7_ = bf16[32,1024]{1,0:T(8,128)(2,1)S(1)} collective-permute-done((bf16[32,1024]{1,0:T(8,128)(2,1)S(1)}, bf16[32,1024]{1,0:T(8,128)(2,1)S(1)}, u32[]{:S(2)}, u32[]{:S(2)}) %collective-permute-start.14) | collective-permute-done | bytes 65568 | tf_op jit(solution)/shard_map/ppermute | solution.py:39
  63.6 0.8 %combine.1 = bf16[32,1024]{1,0:T(8,128)(2,1)} custom-call(f32[8,128]{1,0:T(8,128)S(1)} %opening.1.zero, f32[32,128]{1,0:T(8,128)S(1)} %shares.1.share, bf16[128,1024]{1,0:T(8,128)(2,1)S(1)} %add_convert_fusion.1.refs_0_, bf16[32,1024]{1,0:T(8,128)(2,1)S(1)} %collective-permute-done.5.refs_1_, bf16[32,1024]{1,0:T(8,128)(2,1)S(1)} %collective-permute-done.6.refs_2_, ...), custom_call_target="tpu_custom_call" | custom-call | tf_op jit(solution)/shard_map/combine/pallas_call | solution.py:201
  (43 shorter events, 4.5 us)
Async XLA Ops:
  0.0 6.6 %collective-permute-start = (bf16[32,1024]{1,0:T(8,128)(2,1)}, bf16[32,1024]{1,0:T(8,128)(2,1)S(1)}, u32[]{:S(2)}, u32[]{:S(2)}) collective-permute-start(bf16[32,1024]{1,0:T(8,128)(2,1)} %param.7), channel_id=1, source_target_pairs={{0,4},{2,6},{4,0},{6,2},{8,12},{10,14},{12,8},{14,10},{1,5},{3,7},... | collective-permute-start | bytes 196616 | tf_op jit(solution)/shard_map/ppermute | solution.py:39
  3.1 7.5 %collective-permute-start.1 = (bf16[32,1024]{1,0:T(8,128)(2,1)}, bf16[32,1024]{1,0:T(8,128)(2,1)S(1)}, u32[]{:S(2)}, u32[]{:S(2)}) collective-permute-start(bf16[32,1024]{1,0:T(8,128)(2,1)} %param.7), channel_id=1, source_target_pairs={{0,8},{2,10},{4,12},{6,14},{8,0},{10,2},{12,4},{14,6},{1,9},{3,11}... | collective-permute-start | bytes 196616 | tf_op jit(solution)/shard_map/ppermute | solution.py:39
  5.6 6.3 %collective-permute-start.2 = (bf16[32,1024]{1,0:T(8,128)(2,1)}, bf16[32,1024]{1,0:T(8,128)(2,1)S(1)}, u32[]{:S(2)}, u32[]{:S(2)}) collective-permute-start(bf16[32,1024]{1,0:T(8,128)(2,1)} %param.7), channel_id=1, source_target_pairs={{0,12},{2,14},{4,8},{6,10},{8,4},{10,6},{12,0},{14,2},{1,13},{3,15... | collective-permute-start | bytes 196616 | tf_op jit(solution)/shard_map/ppermute | solution.py:39
  6.6 25.3 %slice-start = ((s8[12582912]{0:T(1024)(128)(4,1)}), s8[4194304]{0:T(1024)(128)(4,1)S(1)}, s32[]{:S(2)}) async-start(s8[12582912]{0:T(1024)(128)(4,1)} %bitcast.6), calls=%async_computation | async-start | bytes 8388608
  12.0 6.4 %collective-permute-start.8 = (bf16[128,1024]{1,0:T(8,128)(2,1)S(1)}, bf16[128,1024]{1,0:T(8,128)(2,1)S(1)}, u32[]{:S(2)}, u32[]{:S(2)}) collective-permute-start(bf16[128,1024]{1,0:T(8,128)(2,1)S(1)} %constant_dynamic-update-slice_fusion.refs_0_), channel_id=1, source_target_pairs={{0,2},{2,0},{4,6},{6,4},{8,10},{10,8},{12,14},{14,12},{1,3},{3,1},... | collective-permute-start | bytes 786440 | tf_op jit(solution)/shard_map/ppermute | solution.py:39
  13.4 4.9 %collective-permute-start.3 = (bf16[128,1024]{1,0:T(8,128)(2,1)S(1)}, bf16[128,1024]{1,0:T(8,128)(2,1)S(1)}, u32[]{:S(2)}, u32[]{:S(2)}) collective-permute-start(bf16[128,1024]{1,0:T(8,128)(2,1)S(1)} %constant_dynamic-update-slice_fusion.refs_0_), channel_id=1, source_target_pairs={{0,1},{1,0},{2,3},{3,2},{4,5},{5,4},{6,7},{7,6},{8,9},{9,8},{10,11... | collective-permute-start | bytes 786440 | tf_op jit(solution)/shard_map/ppermute | solution.py:39
  18.4 16.2 %collective-permute-start.9 = (bf16[128,1024]{1,0:T(8,128)(2,1)S(1)}, bf16[128,1024]{1,0:T(8,128)(2,1)S(1)}, u32[]{:S(2)}, u32[]{:S(2)}) collective-permute-start(bf16[128,1024]{1,0:T(8,128)(2,1)S(1)} %collective-permute-done.8.refs_0_), channel_id=1, source_target_pairs={{0,1},{1,0},{2,3},{3,2},{4,5},{5,4},{6,7},{7,6},{8,9},{9,8},{10,11... | collective-permute-start | bytes 786440 | tf_op jit(solution)/shard_map/ppermute | solution.py:39
  18.4 4.6 %copy-start = (bf16[1,2048,3072]{2,1,0:T(8,128)(2,1)S(1)}, bf16[1,2048,3072]{2,1,0:T(8,128)(2,1)}, u32[]{:S(2)}) copy-start(bf16[1,2048,3072]{2,1,0:T(8,128)(2,1)} %param.11) | copy-start | bytes 37748740
  22.9 4.6 %copy-start.1 = (bf16[1,2048,3072]{2,1,0:T(8,128)(2,1)S(1)}, bf16[1,2048,3072]{2,1,0:T(8,128)(2,1)}, u32[]{:S(2)}) copy-start(bf16[1,2048,3072]{2,1,0:T(8,128)(2,1)} %param.12) | copy-start | bytes 37748740
  27.5 4.4 %slice-start.1 = ((s8[12582912]{0:T(1024)(128)(4,1)}), s8[4194304]{0:T(1024)(128)(4,1)S(1)}, s32[]{:S(2)}) async-start(s8[12582912]{0:T(1024)(128)(4,1)} %bitcast.6), calls=%async_computation.1 | async-start | bytes 8388608
  27.5 4.4 %slice-start.2 = ((s8[12582912]{0:T(1024)(128)(4,1)}), s8[4194304]{0:T(1024)(128)(4,1)S(1)}, s32[]{:S(2)}) async-start(s8[12582912]{0:T(1024)(128)(4,1)} %bitcast.6), calls=%async_computation.2 | async-start | bytes 8388608
  31.9 2.7 %slice-start.3 = ((s8[12582912]{0:T(1024)(128)(4,1)}), s8[4194304]{0:T(1024)(128)(4,1)S(1)}, s32[]{:S(2)}) async-start(s8[12582912]{0:T(1024)(128)(4,1)} %bitcast.13), calls=%async_computation.3 | async-start | bytes 8388608
  31.9 3.5 %slice-start.4 = ((s8[12582912]{0:T(1024)(128)(4,1)}), s8[4194304]{0:T(1024)(128)(4,1)S(1)}, s32[]{:S(2)}) async-start(s8[12582912]{0:T(1024)(128)(4,1)} %bitcast.13), calls=%async_computation.4 | async-start | bytes 8388608
  31.9 7.1 %copy-start.2 = (bf16[1,2048,3072]{2,1,0:T(8,128)(2,1)S(1)}, bf16[1,2048,3072]{2,1,0:T(8,128)(2,1)}, u32[]{:S(2)}) copy-start(bf16[1,2048,3072]{2,1,0:T(8,128)(2,1)} %param.12) | copy-start | bytes 37748740
  33.0 7.4 %slice-start.5 = ((s8[12582912]{0:T(1024)(128)(4,1)}), s8[4194304]{0:T(1024)(128)(4,1)S(1)}, s32[]{:S(2)}) async-start(s8[12582912]{0:T(1024)(128)(4,1)} %bitcast.13), calls=%async_computation.5 | async-start | bytes 8388608
  33.0 13.2 %collective-permute-start.4 = (bf16[128,1024]{1,0:T(8,128)(2,1)S(1)}, bf16[128,1024]{1,0:T(8,128)(2,1)S(1)}, u32[]{:S(2)}, u32[]{:S(2)}) collective-permute-start(bf16[128,1024]{1,0:T(8,128)(2,1)S(1)} %down.5), channel_id=1, source_target_pairs={{0,1},{1,0},{2,3},{3,2},{4,5},{5,4},{6,7},{7,6},{8,9},{9,8},{10,11... | collective-permute-start | bytes 786440 | tf_op jit(solution)/shard_map/ppermute | solution.py:39
  45.6 6.1 %collective-permute-start.10 = (bf16[128,1024]{1,0:T(8,128)(2,1)S(1)}, bf16[128,1024]{1,0:T(8,128)(2,1)S(1)}, u32[]{:S(2)}, u32[]{:S(2)}) collective-permute-start(bf16[128,1024]{1,0:T(8,128)(2,1)S(1)} %down.7), channel_id=1, source_target_pairs={{0,1},{1,0},{2,3},{3,2},{4,5},{5,4},{6,7},{7,6},{8,9},{9,8},{10,11... | collective-permute-start | bytes 786440 | tf_op jit(solution)/shard_map/ppermute | solution.py:39
  46.3 7.1 %collective-permute-start.5 = (bf16[32,1024]{1,0:T(8,128)(2,1)S(1)}, bf16[32,1024]{1,0:T(8,128)(2,1)S(1)}, u32[]{:S(2)}, u32[]{:S(2)}) collective-permute-start(bf16[32,1024]{1,0:T(8,128)(2,1)S(1)} %get-tuple-element.11), channel_id=1, source_target_pairs={{0,4},{2,6},{4,0},{6,2},{8,12},{10,14},{12,8},{14,10},{1,5},{3,7},... | collective-permute-start | bytes 196616 | tf_op jit(solution)/shard_map/ppermute | solution.py:39
  47.1 9.6 %collective-permute-start.6 = (bf16[32,1024]{1,0:T(8,128)(2,1)S(1)}, bf16[32,1024]{1,0:T(8,128)(2,1)S(1)}, u32[]{:S(2)}, u32[]{:S(2)}) collective-permute-start(bf16[32,1024]{1,0:T(8,128)(2,1)S(1)} %get-tuple-element.10), channel_id=1, source_target_pairs={{0,8},{2,10},{4,12},{6,14},{8,0},{10,2},{12,4},{14,6},{1,9},{3,11}... | collective-permute-start | bytes 196616 | tf_op jit(solution)/shard_map/ppermute | solution.py:39
  48.7 10.8 %collective-permute-start.7 = (bf16[32,1024]{1,0:T(8,128)(2,1)S(1)}, bf16[32,1024]{1,0:T(8,128)(2,1)S(1)}, u32[]{:S(2)}, u32[]{:S(2)}) collective-permute-start(bf16[32,1024]{1,0:T(8,128)(2,1)S(1)} %get-tuple-element.9), channel_id=1, source_target_pairs={{0,12},{2,14},{4,8},{6,10},{8,4},{10,6},{12,0},{14,2},{1,13},{3,15... | collective-permute-start | bytes 196616 | tf_op jit(solution)/shard_map/ppermute | solution.py:39
  51.8 7.6 %collective-permute-start.11 = (bf16[32,1024]{1,0:T(8,128)(2,1)S(1)}, bf16[32,1024]{1,0:T(8,128)(2,1)S(1)}, u32[]{:S(2)}, u32[]{:S(2)}) collective-permute-start(bf16[32,1024]{1,0:T(8,128)(2,1)S(1)} %get-tuple-element.8), channel_id=1, source_target_pairs={{0,2},{2,0},{4,6},{6,4},{8,10},{10,8},{12,14},{14,12},{1,3},{3,1},... | collective-permute-start | bytes 196616 | tf_op jit(solution)/shard_map/ppermute | solution.py:39
  53.4 6.1 %collective-permute-start.12 = (bf16[32,1024]{1,0:T(8,128)(2,1)S(1)}, bf16[32,1024]{1,0:T(8,128)(2,1)S(1)}, u32[]{:S(2)}, u32[]{:S(2)}) collective-permute-start(bf16[32,1024]{1,0:T(8,128)(2,1)S(1)} %get-tuple-element.7), channel_id=1, source_target_pairs={{0,6},{2,4},{4,2},{6,0},{8,14},{10,12},{12,10},{14,8},{1,7},{3,5},... | collective-permute-start | bytes 196616 | tf_op jit(solution)/shard_map/ppermute | solution.py:39
  53.4 6.8 %collective-permute-start.13 = (bf16[32,1024]{1,0:T(8,128)(2,1)S(1)}, bf16[32,1024]{1,0:T(8,128)(2,1)S(1)}, u32[]{:S(2)}, u32[]{:S(2)}) collective-permute-start(bf16[32,1024]{1,0:T(8,128)(2,1)S(1)} %get-tuple-element.6), channel_id=1, source_target_pairs={{0,10},{2,8},{4,14},{6,12},{8,2},{10,0},{12,6},{14,4},{1,11},{3,9}... | collective-permute-start | bytes 196616 | tf_op jit(solution)/shard_map/ppermute | solution.py:39
  56.7 7.0 %collective-permute-start.14 = (bf16[32,1024]{1,0:T(8,128)(2,1)S(1)}, bf16[32,1024]{1,0:T(8,128)(2,1)S(1)}, u32[]{:S(2)}, u32[]{:S(2)}) collective-permute-start(bf16[32,1024]{1,0:T(8,128)(2,1)S(1)} %get-tuple-element.5), channel_id=1, source_target_pairs={{0,14},{2,12},{4,10},{6,8},{8,6},{10,4},{12,2},{14,0},{1,15},{3,13... | collective-permute-start | bytes 196616 | tf_op jit(solution)/shard_map/ppermute | solution.py:39
